TPU v7x, 512 devices: a whole 4x4x16 slice. The times are simulated.
512 devices in a mesh: dp: 4 (over x), kv: 64 (over z, y), tp: 2 (over core).
Axes of the slice: x: 4, y: 4, z: 16, core: 2. Of those that a mesh axis runs over, the one named last changes fastest.
Arguments:
- tokens: bfloat16 [512, 4, 2048], P('dp', None, 'kv'), may hold values from -600 to 600
- input_norm_gain: float32 [2048], P('kv'), may hold values from 0.1 to 1.9
- query_projection: bfloat16 [2048, 1024], P('kv', 'tp'), may hold values from -0.125 to 0.125
- key_projection: bfloat16 [2048, 1024], P('kv', 'tp'), may hold values from -0.125 to 0.125
- value_projection: bfloat16 [2048, 1024], P('kv', 'tp'), may hold values from -0.125 to 0.125
- write_strength_weight: bfloat16 [2048, 16], P('kv', 'tp'), may hold values from -0.125 to 0.125
- decay_projection: bfloat16 [2048, 16], P('kv', 'tp'), may hold values from -0.125 to 0.125
- head_decay_rate: float32 [16], P('tp'), may hold values from 0.02 to 0.6
- token_extra_decay: float32 [512, 4, 16], P(('dp', 'kv'), None, 'tp'), may hold values from -0.7 to 0
- accepted: int32 [512], P(('dp', 'kv')), may hold values from 1 to 4
- prior_step_states: float32 [512, 4, 16, 4096], P(('dp', 'kv'), None, 'tp'), may hold values from -4 to 4
- output_norm_gain: float32 [64], replicated, may hold values from 0.1 to 1.9
- output_projection: bfloat16 [1024, 2048], P('tp', 'kv'), may hold values from -0.1875 to 0.1875
Outputs:
- mixed: bfloat16 [512, 4, 2048], P('dp', None, 'kv')
- updated_states: float32 [512, 4, 16, 4096], P(('dp', 'kv'), None, 'tp')
Inputs may be any that keep to these rules, and one draw needn't show every extreme that they name: `accepted`: how many proposals of the previous step each sequence kept; its state after that many is taken up.
All inputs are finite; a program needn't handle non-finite values.
Results may differ from a plain program's by a relative error of at most 0.029.
Values may be sent and summed in bfloat16 or wider, within the bound.
No kernel may reach another device: no remote copies, remote signals or barrier semaphores. Data moves between devices by JAX's collectives and lax.ppermute only.
A program may use at most 64 MiB of HBM per device.

v0:
```python
import jax
import jax.numpy as jnp
from jax import lax
from jax.sharding import Mesh
from jax.sharding import PartitionSpec as P

D = 2048
KV = ("kv_0", "kv_1")
DP_KV = ("dp", "kv_0", "kv_1")


epsilon = 1e-06
highest = lax.Precision.HIGHEST


def cut_along(x, dim, length):
    before, after = (x.shape[:dim], x.shape[dim + 1 :])
    return jnp.moveaxis(x.reshape(*before, length, -1, *after), dim, 0)


def summed_on_arrival(x, axis, dim):
    tiles = cut_along(x, dim, lax.axis_size(axis))
    arrived = lax.all_to_all(tiles, axis, split_axis=0, concat_axis=0, tiled=True)
    return arrived.sum(axis=0)


def sum_in_two_steps(x, axes, dim):
    far, near = axes
    tiles = cut_along(x, dim, lax.axis_size(far))
    nearer = summed_on_arrival(tiles, near, dim + 1)
    arrived = lax.all_to_all(nearer, far, split_axis=0, concat_axis=0, tiled=True)
    return arrived.sum(axis=0)


def side_by_side(arrays, axis, dim, along):
    columns = [a.reshape(*a.shape[:along], -1) for a in arrays]
    both = jnp.concatenate(columns, axis=along)
    whole, at, done = (sum_in_two_steps(both, axis, dim), 0, [])
    for a, column in zip(arrays, columns):
        share = whole[..., at : at + column.shape[along]]
        done.append(share.reshape(*share.shape[:along], *a.shape[along:]))
        at += column.shape[along]
    return tuple(done)


def gather_axes(x, axes, dim):
    whole = x
    for number in range(len(axes) - 1, -1, -1):
        whole = lax.all_gather(whole, axes[number], axis=dim, tiled=True)
    return whole


def sent_to_all(x, axis):
    length = lax.axis_size(axis)
    return lax.all_to_all(jnp.broadcast_to(x[None], (length, *x.shape)), axis, 0, 0, tiled=True)


def of_everyone(x, axis):
    everything = sent_to_all(x, axis)
    return jnp.sum(everything.astype(jnp.float32), axis=0)


def unit_rows(values):
    return values * lax.rsqrt(jnp.sum(values * values, axis=-1, keepdims=True) + epsilon)


def delta_block(query_heads, key_heads, value_heads, beta_gate, decay_logarithm, start_state):
    proposal_len = query_heads.shape[2]
    cumulative = jnp.cumsum(decay_logarithm, axis=-1)
    spread = cumulative[..., :, None] - cumulative[..., None, :]
    strict = jnp.tril(jnp.ones((proposal_len, proposal_len), bool), -1)
    inclusive = jnp.tril(jnp.ones((proposal_len, proposal_len), bool))
    key_inner = jnp.einsum("nhid,nhjd->nhij", key_heads, key_heads, precision=highest)
    coupling = jnp.where(
        strict, beta_gate[..., :, None] * key_inner * jnp.exp(jnp.where(strict, spread, 0.0)), 0.0
    )
    growth = jnp.exp(cumulative)
    right_w = (beta_gate * growth)[..., None] * key_heads
    right_u = beta_gate[..., None] * value_heads
    solved_w = []
    solved_u = []
    for current in range(proposal_len):
        part_w = right_w[:, :, current]
        part_u = right_u[:, :, current]
        for earlier in range(current):
            factor = coupling[:, :, current, earlier][..., None]
            part_w = part_w - factor * solved_w[earlier]
            part_u = part_u - factor * solved_u[earlier]
        solved_w.append(part_w)
        solved_u.append(part_u)
    weights_w = jnp.stack(solved_w, axis=2)
    weights_u = jnp.stack(solved_u, axis=2)
    corrected = weights_u - jnp.einsum("nhpd,nhde->nhpe", weights_w, start_state, precision=highest)
    within = jnp.where(inclusive, jnp.exp(jnp.where(inclusive, spread, 0.0)), 0.0)
    scores = jnp.einsum("nhid,nhjd->nhij", query_heads, key_heads, precision=highest) * within
    attended = jnp.einsum(
        "nhpd,nhde->nhpe", query_heads * growth[..., None], start_state, precision=highest
    ) + jnp.einsum("nhij,nhje->nhie", scores, corrected, precision=highest)
    states = growth[..., None, None] * start_state[:, :, None] + jnp.einsum(
        "nhtj,nhjd,nhje->nhtde", within, key_heads, corrected, precision=highest
    )
    return (attended, states)


def combine_heads(
    query_logits,
    key_logits,
    value_logits,
    beta_logits,
    decay_logits,
    head_decay_rate,
    token_extra_decay,
    accepted,
    prior_step_states,
    output_norm_gain,
):
    seq_count, proposal_len, head_count = beta_logits.shape
    head_size = query_logits.shape[-1] // head_count

    def by_heads(values):
        return jnp.transpose(
            values.reshape(seq_count, proposal_len, head_count, head_size), (0, 2, 1, 3)
        )

    query_heads = unit_rows(by_heads(jax.nn.silu(query_logits))) * head_size ** (-0.5)
    key_heads = unit_rows(by_heads(jax.nn.silu(key_logits)))
    value_heads = by_heads(jax.nn.silu(value_logits))
    beta_gate = jnp.transpose(jax.nn.sigmoid(beta_logits), (0, 2, 1))
    decay_logarithm = jnp.transpose(
        -head_decay_rate[None, None, :] * jax.nn.softplus(decay_logits) + token_extra_decay,
        (0, 2, 1),
    )
    chosen = jnp.arange(proposal_len, dtype=jnp.int32)[None, :] == (accepted - 1)[:, None]
    picked = jnp.sum(jnp.where(chosen[:, :, None, None], prior_step_states, 0.0), axis=1)
    start_state = picked.reshape(seq_count, head_count, head_size, head_size)
    attended, states = delta_block(
        query_heads, key_heads, value_heads, beta_gate, decay_logarithm, start_state
    )
    inverse_rms = lax.rsqrt(jnp.mean(attended * attended, axis=-1, keepdims=True) + epsilon)
    normalized_rows = (attended * inverse_rms * output_norm_gain).astype(jnp.bfloat16)
    normalized_rows = jnp.transpose(normalized_rows, (0, 2, 1, 3)).reshape(
        seq_count, proposal_len, head_count * head_size
    )
    updated_states = jnp.transpose(states, (0, 2, 1, 3, 4)).reshape(
        seq_count, proposal_len, head_count, head_size * head_size
    )
    return (normalized_rows, updated_states)


def per_device(
    tokens,
    input_norm_gain,
    query_projection,
    key_projection,
    value_projection,
    write_strength_weight,
    decay_projection,
    head_decay_rate,
    token_extra_decay,
    accepted,
    prior_step_states,
    output_norm_gain,
    output_projection,
):
    group_seqs, proposal_len, feature_dev = tokens.shape
    own_seqs = prior_step_states.shape[0]
    own_rows = own_seqs * proposal_len
    token_rows = tokens.reshape(group_seqs * proposal_len, feature_dev).astype(jnp.float32)
    squares = jnp.sum(token_rows * token_rows, axis=1)
    scaled = (token_rows * input_norm_gain[None, :]).astype(jnp.bfloat16)
    part_query = jnp.dot(scaled, query_projection, preferred_element_type=jnp.float32)
    part_key = jnp.dot(scaled, key_projection, preferred_element_type=jnp.float32)
    part_value = jnp.dot(scaled, value_projection, preferred_element_type=jnp.float32)
    part_beta = jnp.dot(scaled, write_strength_weight, preferred_element_type=jnp.float32)
    part_decay = jnp.dot(scaled, decay_projection, preferred_element_type=jnp.float32)
    summed = side_by_side(
        (part_query, part_key, part_value, part_beta, part_decay, squares), ("kv_0", "kv_1"), 0, 1
    )
    query_sum, key_sum, value_sum, beta_sum, decay_sum, square_sum = summed
    inverse = lax.rsqrt(square_sum / D + epsilon)[:, None]

    def own_form(values):
        return (values * inverse).reshape(own_seqs, proposal_len, values.shape[1])

    normalized_rows, updated_states = combine_heads(
        own_form(query_sum),
        own_form(key_sum),
        own_form(value_sum),
        own_form(beta_sum),
        own_form(decay_sum),
        head_decay_rate,
        token_extra_decay,
        accepted,
        prior_step_states,
        output_norm_gain,
    )
    normed_rows = normalized_rows.reshape(own_rows, normalized_rows.shape[2])
    partial_value = jnp.dot(
        gather_axes(normed_rows, KV, 0), output_projection, preferred_element_type=jnp.float32
    )
    mixed = of_everyone(partial_value.astype(jnp.bfloat16), "tp").astype(jnp.float32)
    mixed = mixed.astype(jnp.bfloat16).reshape(group_seqs, proposal_len, output_projection.shape[1])
    return (mixed, updated_states)


def solution(mesh):
    split = Mesh(
        mesh.devices.reshape(mesh.shape["dp"], 16, 4, mesh.shape["tp"]),
        ("dp", "kv_0", "kv_1", "tp"),
    )
    in_specs = (
        P("dp", None, KV),
        P(KV),
        P(KV, "tp"),
        P(KV, "tp"),
        P(KV, "tp"),
        P(KV, "tp"),
        P(KV, "tp"),
        P("tp"),
        P(DP_KV, None, "tp"),
        P(DP_KV),
        P(DP_KV, None, "tp", None),
        P(),
        P("tp", KV),
    )
    out_specs = (P("dp", None, KV), P(DP_KV, None, "tp", None))
    return jax.shard_map(
        per_device, mesh=split, in_specs=in_specs, out_specs=out_specs, check_vma=False
    )
```

profile of v0, /device:TPU:1, one launch (start us, length us, event | category | flops | bytes accessed | tf_op | source)
XLA Modules:
  0.0 180.3 jit_solution(13464911066317285011)
XLA Ops:
  0.7 0.9 copy.181
  1.6 0.8 multiply_reduce_fusion
  2.3 0.7 multiply_convert_fusion
  3.1 1.3 fusion.11
  4.3 2.0 %fusion.13 = f32[16,4,8,512]{3,2,1,0:T(8,128)} fusion(bf16[16,4,8,32]{3,2,1,0:T(8,128)(2,1)S(1)} %multiply_convert_fusion, bf16[32,512]{1,0:T(8,128)(2,1)} %param.15), kind=kOutput, calls=%fused_computation.25 | convolution fusion | flops 16777216 | bytes 1114112 | tf_op jit(solution)/shard_map/dot_general | solution.py:171
  6.3 1.3 fusion.9
  7.6 0.9 fusion.44
  8.5 0.9 fusion.46
  9.4 0.1 copy.184
  9.5 0.8 concatenate.8
  10.3 2.9 %concatenate.7 = f32[16,4,8,1553]{3,2,1,0:T(8,128)S(1)} concatenate(f32[16,4,8,512]{3,2,1,0:T(8,128)} %fusion.13, f32[16,4,8,512]{3,2,1,0:T(8,128)} %fusion.11, f32[16,4,8,512]{3,2,1,0:T(8,128)} %fusion.9, f32[16,4,8,8]{3,2,1,0:T(8,128)} %fusion.46, f32[16,4,8,8]{3,2,1,0:T(8,128)} %fusion.44, f32[16,4,8,1]{3,2,1,0:T(8,128)} %concatenate.8), dimensions={3} | concatenate | bytes 6361088 | tf_op jit(solution)/shard_map/concatenate | solution.py:37
  13.2 0.2 copy.188
  13.4 40.7 %all_to_all.15 = f32[4,16,8,1553]{3,2,1,0:T(8,128)S(1)} all-to-all(f32[4,16,8,1553]{3,2,1,0:T(8,128)S(1)} %copy.188), channel_id=1, replica_groups=mesh['dp'=4,'kv_0'=16,'kv_1'=4,'tp'=2] {'kv_1'}, dimensions={0} | all-to-all | bytes 6361088 | tf_op jit(solution)/shard_map/all_to_all | solution.py:23
  54.1 1.2 reduce_sum.76
  55.3 18.6 %all-to-all-start.1 = ((f32[16,8,1553]{2,1,0:T(8,128)}), f32[16,8,1553]{2,1,0:T(8,128)S(1)}, u32[]{:S(2)}, u32[]{:S(2)}) async-start(f32[16,8,1553]{2,1,0:T(8,128)} %reduce_sum.76), calls=%async_computation.1 | async-start | bytes 1703936 | tf_op jit(solution)/shard_map/all_to_all | solution.py:31
  74.1 0.1 select_reduce_fusion
  74.2 0.2 reshape.147
  74.5 37.2 %all-to-all-done.1 = f32[16,8,1553]{2,1,0:T(8,128)S(1)} async-done(((f32[16,8,1553]{2,1,0:T(8,128)}), f32[16,8,1553]{2,1,0:T(8,128)S(1)}, u32[]{:S(2)}, u32[]{:S(2)}) %all-to-all-start.1) | async-done | bytes 795168 | tf_op jit(solution)/shard_map/all_to_all | solution.py:31
  111.8 0.2 fusion.43
  112.0 0.1 fusion.40
  112.2 0.1 copy.192
  112.3 0.1 copy.194
  112.5 0.1 fusion.18
  112.7 0.1 fusion.19
  112.8 0.1 fusion.26
  112.9 0.3 fusion.1
  113.2 0.3 slice_reduce_fusion.4
  113.6 0.1 bitcast_multiply_fusion.1
  113.7 0.1 fusion.29
  113.8 0.5 fusion.21
  114.4 0.1 copy.204
  114.5 0.1 fusion.7
  114.6 3.7 %bitcast_add_fusion = f32[2,4,8,64,64]{4,3,1,2,0:T(8,128)S(1)} fusion(f32[2,8,64,64]{3,2,1,0:T(8,128)S(1)} %reshape.147, f32[2,4,8]{1,2,0:T(8,128)S(1)} %copy.204, f32[2,8,4,4]{2,3,1,0:T(4,128)S(1)} %fusion.7, f32[2,8,4,64]{3,2,1,0:T(4,128)S(1)} %copy.191, f32[2,8,4,64,1]{3,1,2,0,4:T(8,128)S(1)} %fusion.60), kind=kOutput, calls=%fused_computation | convolution fusion | flops 13123584 | bytes 1344768 | tf_op jit(solution)/shard_map/nhtj,nhjd,nhje->nhtde/dot_general | solution.py:99
  118.3 1.8 %reshape.151 = f32[2,4,8,4096]{3,1,2,0:T(4,128)} reshape(f32[2,4,8,64,64]{4,3,1,2,0:T(8,128)S(1)} %bitcast_add_fusion) | data formatting | bytes 2097152 | tf_op jit(solution)/shard_map/reshape | solution.py:144
  120.1 2.8 %copy.208 = f32[2,4,8,4096]{3,2,1,0:T(8,128)} copy(f32[2,4,8,4096]{3,1,2,0:T(4,128)} %reshape.151) | data formatting | bytes 2097152
  122.9 0.3 convolution_multiply_fusion.1
  123.2 0.5 fusion.24
  123.7 0.3 multiply_reduce_fusion.1
  124.1 0.1 copy.221
  124.1 0.1 copy.201
  124.2 0.1 fusion.17
  124.3 0.1 reshape_reshape.4
  124.4 9.0 %all_gather.6 = bf16[32,512]{1,0:T(8,128)(2,1)S(1)} all-gather(bf16[8,512]{1,0:T(8,128)(2,1)S(1)} %reshape_reshape.4), channel_id=1, replica_groups=mesh['dp'=4,'kv_0'=16,'kv_1'=4,'tp'=2] {'kv_1'}, dimensions={0}, use_global_device_ids=true | all-gather | bytes 40960 | tf_op jit(solution)/shard_map/all_gather | solution.py:49
  133.5 27.0 %all_gather.7 = bf16[512,512]{1,0:T(8,128)(2,1)S(1)} all-gather(bf16[32,512]{1,0:T(8,128)(2,1)S(1)} %all_gather.6), channel_id=1, replica_groups=mesh['dp'=4,'kv_0'=16,'kv_1'=4,'tp'=2] {'kv_0'}, dimensions={0}, use_global_device_ids=true | all-gather | bytes 557056 | tf_op jit(solution)/shard_map/all_gather | solution.py:49
  160.4 0.2 convolution_convert_fusion
  160.7 18.7 %all_to_all.16 = bf16[2,512,32]{1,2,0:T(8,128)(2,1)S(1)} all-to-all(bf16[2,512,32]{1,2,0:T(8,128)(2,1)S(1)} %broadcast_in_dim.60), channel_id=1, replica_groups=mesh['dp'=4,'kv_0'=16,'kv_1'=4,'tp'=2] {'tp'}, dimensions={0} | all-to-all | bytes 131072 | tf_op jit(solution)/shard_map/all_to_all | solution.py:55
  179.5 0.1 copy.203
  179.6 0.7 copy.207
  (45 shorter events, 0.8 us)
Async XLA Ops:
  0.6 2.4 %copy-start = (bf16[32,512]{1,0:T(8,128)(2,1)S(1)}, bf16[32,512]{1,0:T(8,128)(2,1)}, u32[]{:S(2)}) copy-start(bf16[32,512]{1,0:T(8,128)(2,1)} %param.16) | copy-start | bytes 98308
  0.6 5.7 %copy-start.2 = (bf16[32,512]{1,0:T(8,128)(2,1)S(1)}, bf16[32,512]{1,0:T(8,128)(2,1)}, u32[]{:S(2)}) copy-start(bf16[32,512]{1,0:T(8,128)(2,1)} %param.17) | copy-start | bytes 98308
  1.6 6.1 %copy-start.5 = (bf16[32,8]{0,1:T(8,128)(2,1)S(1)}, bf16[32,8]{0,1:T(8,128)(2,1)}, u32[]{:S(2)}) copy-start(bf16[32,8]{0,1:T(8,128)(2,1)} %param.19) | copy-start | bytes 1540
  3.0 5.4 %copy-start.6 = (bf16[32,8]{0,1:T(8,128)(2,1)S(1)}, bf16[32,8]{0,1:T(8,128)(2,1)}, u32[]{:S(2)}) copy-start(bf16[32,8]{0,1:T(8,128)(2,1)} %param.18) | copy-start | bytes 1540
  54.1 19.8 %copy-start.8 = (f32[8]{0:T(128)S(1)}, f32[8]{0:T(128)}, u32[]{:S(2)}) copy-start(f32[8]{0:T(128)} %param.20) | copy-start | bytes 100
  54.1 19.8 %copy-start.9 = (s32[2]{0:T(128)S(1)}, s32[2]{0:T(128)}, u32[]{:S(2)}) copy-start(s32[2]{0:T(128)} %param.22) | copy-start | bytes 28
  55.3 18.8 %copy-start.1 = (f32[2,4,8,4096]{3,2,1,0:T(8,128)S(1)}, f32[2,4,8,4096]{3,2,1,0:T(8,128)}, u32[]{:S(2)}) copy-start(f32[2,4,8,4096]{3,2,1,0:T(8,128)} %param.23) | copy-start | bytes 3145732
  55.3 56.9 %copy-start.4 = (f32[2,4,8]{2,1,0:T(4,128)S(1)}, f32[2,4,8]{2,1,0:T(4,128)}, u32[]{:S(2)}) copy-start(f32[2,4,8]{2,1,0:T(4,128)} %param.21) | copy-start | bytes 772
  55.3 56.5 %all-to-all-start.1 = ((f32[16,8,1553]{2,1,0:T(8,128)}), f32[16,8,1553]{2,1,0:T(8,128)S(1)}, u32[]{:S(2)}, u32[]{:S(2)}) async-start(f32[16,8,1553]{2,1,0:T(8,128)} %reduce_sum.76), calls=%async_computation.1 | async-start | bytes 1703936 | tf_op jit(solution)/shard_map/all_to_all | solution.py:31
  120.1 4.1 %copy-start.7 = (f32[64]{0:T(128)S(1)}, f32[64]{0:T(128)}, u32[]{:S(2)}) copy-start(f32[64]{0:T(128)} %param.24) | copy-start | bytes 772
  120.1 40.3 %copy-start.3 = (bf16[512,32]{0,1:T(8,128)(2,1)S(1)}, bf16[512,32]{0,1:T(8,128)(2,1)}, u32[]{:S(2)}) copy-start(bf16[512,32]{0,1:T(8,128)(2,1)} %param.25) | copy-start | bytes 98308
where the time goes:
time: 181 us; the launch traced here: 180 us
  blocking collectives  95.4 us (53%)
  waiting for transfers between devices  37.2 us (21%)
  starting transfers between devices  18.6 us (10%)
  matrix products  12.1 us (7%)
  local copies, waits for them, and re-layouts  11.8 us (7%)
  other arithmetic  4.17 us (2%)
    all_to_all x1, blocking collectives, summed_on_arrival(): lax.all_to_all(tiles, axis, split_axis=0, concat_axis=0, tiled=True)  40.7 us
    all_to_all x1, waiting for transfers between devices, sum_in_two_steps(): lax.all_to_all(nearer, far, split_axis=0, concat_axis=0, tiled=True)  37.2 us
    all_gather x2, blocking collectives, gather_axes(): whole = lax.all_gather(whole, axes[number], axis=dim, tiled=True)  36 us
    all_to_all x1, blocking collectives, sent_to_all(): lax.all_to_all(jnp.broadcast_to(x[None], (length, *x.shape)), axis, 0, 0,...  18.7 us
    all_to_all x1, starting transfers between devices, sum_in_two_steps(): lax.all_to_all(nearer, far, split_axis=0, concat_axis=0, tiled=True)  18.6 us
    concatenate x2, local copies, waits for them, and re-layouts, side_by_side(): both = jnp.concatenate(columns, axis=along)  3.7 us
    dot_general x1, matrix products, delta_block(): jnp.einsum('nhtj,nhjd,nhje->nhtde', within, key_heads, corrected, precisi...  3.69 us
    unnamed x23, local copies, waits for them, and re-layouts  3.68 us
  transfers between devices with their start and end apart: 1, of which 1 were waited for; matrix products, arithmetic and copies ran while one was open for 0% of the time, Pallas kernels for 0%

commit v1 on v0

v1 whole, which is shorter than its diff:
```python
import jax
import jax.numpy as jnp
import numpy as np
from jax import lax
from jax.experimental import pallas as pl
from jax.experimental.pallas import tpu as pltpu
from jax.sharding import Mesh
from jax.sharding import PartitionSpec as P

D = 2048
epsilon = 1e-06
KV = ("z8", "zp", "y")
DP_KV = ("dp", "z8", "zp", "y")
NEAR = ("zp", "y")
f32 = jnp.float32
bf16 = jnp.bfloat16

WO, QKV, SMALL, TOK, WIDE = 0, 512, 2048, 2176, 2304
VMEM = pl.BlockSpec(memory_space=pltpu.VMEM)
SMEM = pl.BlockSpec(memory_space=pltpu.SMEM)


def iota(shape, dim):
    return lax.broadcasted_iota(jnp.int32, shape, dim)


def dot(a, b, ca, cb):
    return lax.dot_general(a, b, (((ca,), (cb,)), ((), ())), preferred_element_type=f32)


def pack_kernel(tok_ref, gain_ref, q_ref, k_ref, v_ref, beta_ref, decay_ref, wo_ref, out_ref):
    eye = iota((32, 32), 0) == iota((32, 32), 1)
    gain = jnp.sum(jnp.where(eye, gain_ref[...], 0.0), axis=1, keepdims=True)
    raw = jnp.concatenate([tok_ref[t] for t in range(4)], axis=1)
    scaled = (raw.astype(f32) * gain).astype(bf16)
    source, dest = iota((512, 512), 0), iota((512, 512), 1)
    group, rho = dest // 64, dest % 64
    wanted = (rho % 4) * 128 + (rho // 8) * 16 + group * 2 + (rho % 8) // 4
    pick = (source == wanted).astype(f32).astype(bf16)
    both = dot(jnp.concatenate([scaled, raw], axis=0), pick, 1, 0)
    head, lane = iota((8, 128), 0), iota((8, 128), 1)
    put_beta = ((lane == head) | (lane == head + 16)).astype(f32).astype(bf16)
    put_decay = ((lane == head + 8) | (lane == head + 24)).astype(f32).astype(bf16)
    small = dot(beta_ref[...], put_beta, 0, 0) + dot(decay_ref[...], put_decay, 0, 0)
    small = small.astype(bf16)
    low = iota((32, 128), 1) < 64
    for r in range(8):
        s = both[:32, 128 * (r // 2) : 128 * (r // 2) + 128]
        w = both[32:, 128 * (r // 2) : 128 * (r // 2) + 128]
        if r % 2 == 0:
            tile = jnp.where(low, s, pltpu.roll(w, 64, 1))
        else:
            tile = jnp.where(low, pltpu.roll(s, 64, 1), w)
        out_ref[r, :, WO:QKV] = wo_ref[...]
        out_ref[r, :, QKV : QKV + 512] = q_ref[...]
        out_ref[r, :, QKV + 512 : QKV + 1024] = k_ref[...]
        out_ref[r, :, QKV + 1024 : SMALL] = v_ref[...]
        out_ref[r, :, SMALL:TOK] = small
        out_ref[r, :, TOK:] = tile.astype(bf16)


def project_kernel(x_ref, out_ref):
    x = x_ref[...].reshape(256, WIDE)
    cols = x[:, TOK:]
    raw = cols.astype(f32)
    square = raw * raw
    high = square.astype(bf16)
    rest = (square - high.astype(f32)).astype(bf16)
    lane = iota((256, 128), 1)
    ones = ((lane == 32) | (lane == 33)).astype(f32).astype(bf16)
    sums = dot(high, ones, 0, 0) + dot(rest, ones, 0, 0)
    main = dot(cols, x[:, QKV:SMALL], 0, 0)
    out_ref[:, : SMALL - QKV] = main[:64].astype(bf16)
    tail = dot(cols, x[:, SMALL:TOK], 0, 0)[:64] + sums[64:]
    first = tail.astype(bf16).astype(f32)
    lane = iota((64, 128), 1)
    keep = (lane < 16) | (lane == 32)
    out_ref[:, SMALL - QKV :] = jnp.where(keep, first, tail - first).astype(bf16)


def delta_kernel(
    accepted_ref, c_ref, prior_ref, rate_ref, extra_ref, gain_ref, states_ref, rows_ref, aux, nrows
):
    c = c_ref[...].astype(f32)
    s = c[0:8]
    for z in range(1, 8):
        s = s + c[8 * z : 8 * z + 8]
    tile = s[:, 1536:]
    total = tile[:, 32:33] + tile[:, 33:34]
    inverse = lax.rsqrt(total / D + epsilon)
    logits = jnp.transpose((tile + pltpu.roll(tile, 112, 1)) * inverse)
    aux[...] = jnp.zeros((8, 128), f32)
    aux[0:4, 0:8] = extra_ref[0]
    aux[4:8, 0:8] = extra_ref[1]
    aux[:, 8:16] = jnp.broadcast_to(rate_ref[...], (8, 8))
    side = jnp.transpose(aux[...])
    beta = jax.nn.sigmoid(logits[0:8])
    fade = jnp.exp(-side[8:16] * jax.nn.softplus(logits[8:16]) + side[0:8])

    sub, lane = iota((8, 128), 0), iota((8, 128), 1)
    masks = [sub == 2 * p + lane // 64 for p in range(4)]
    gain = jnp.concatenate([gain_ref[...], gain_ref[...]], axis=1)

    def silu_of(at):
        u = s[:, at : at + 512] * inverse
        return u / (1.0 + jnp.exp(-u))

    parts = [silu_of(0), silu_of(512), silu_of(1024)]

    def by_heads(values, row):
        m = jnp.zeros((8, 128), f32)
        for p in range(4):
            piece = jnp.broadcast_to(values[row : row + 1, 128 * p : 128 * p + 128], (8, 128))
            m = jnp.where(masks[p], piece, m)
        return m + pltpu.roll(m, 64, 1)

    def unit(values):
        return values * lax.rsqrt(0.5 * jnp.sum(values * values, axis=1, keepdims=True) + epsilon)

    def spread(values, i):
        return jnp.take_along_axis(values, lane // 64 + 2 * i, axis=1, mode="promise_in_bounds")

    for j in range(2):
        start = accepted_ref[j] - 1
        state = [prior_ref[j, start, :, 128 * i : 128 * i + 128] for i in range(32)]
        for t in range(4):
            row = 4 * j + t
            q = unit(by_heads(parts[0], row)) * 0.125
            k = unit(by_heads(parts[1], row))
            v = by_heads(parts[2], row)
            a = jnp.broadcast_to(fade[:, row : row + 1], (8, 128))
            b = jnp.broadcast_to(beta[:, row : row + 1], (8, 128))
            kx = [spread(k, i) for i in range(32)]
            sums = [kx[i] * state[i] for i in range(4)]
            for i in range(4, 32):
                sums[i % 4] = sums[i % 4] + kx[i] * state[i]
            u = (sums[0] + sums[1]) + (sums[2] + sums[3])
            u = u + pltpu.roll(u, 64, 1)
            w = b * (v - a * u)
            sums = [None] * 4
            for i in range(32):
                state[i] = a * state[i] + kx[i] * w
                states_ref[j, t, :, 128 * i : 128 * i + 128] = state[i]
                term = spread(q, i) * state[i]
                sums[i % 4] = term if i < 4 else sums[i % 4] + term
            o = (sums[0] + sums[1]) + (sums[2] + sums[3])
            o = o + pltpu.roll(o, 64, 1)
            mean = jnp.sum(o * o, axis=1, keepdims=True) / 128
            n = o * lax.rsqrt(mean + epsilon) * gain
            for p in range(4):
                nrows[row : row + 1, 128 * p : 128 * p + 128] = jnp.sum(
                    jnp.where(masks[p], n, 0.0), axis=0, keepdims=True
                )
    rows = nrows[...]
    rows_ref[...] = jnp.concatenate([rows] * 8, axis=0).astype(bf16)


def mix_kernel(x_ref, rows_ref, out_ref):
    w = x_ref[:, :, WO:QKV].reshape(256, 512)
    out = dot(w, rows_ref[...], 1, 1).astype(bf16)
    for r in range(8):
        out_ref[2 * r] = out[32 * r : 32 * r + 32]
        out_ref[2 * r + 1] = out[32 * r : 32 * r + 32]


def place_kernel(x_ref, back_ref, out_ref):
    whole = jnp.zeros((32, 512), f32)
    for r in range(8):
        both = (x_ref[2 * r].astype(f32) + x_ref[2 * r + 1].astype(f32)).astype(bf16)
        whole = whole + dot(both, back_ref[64 * r : 64 * r + 64, :], 1, 0)
    for t in range(4):
        out_ref[t] = whole[:, 128 * t : 128 * t + 128].astype(bf16)


def back_table():
    dest = np.arange(512)
    group, rho = dest // 64, dest % 64
    wanted = (rho % 4) * 128 + (rho // 8) * 16 + group * 2 + (rho % 8) // 4
    return (wanted[:, None] == np.arange(512)[None, :]).astype(jnp.bfloat16)


def call(kernel, shapes, args, specs=None, scratch=(), name=None):
    one = not isinstance(shapes, tuple)
    return pl.pallas_call(
        kernel,
        out_shape=shapes,
        in_specs=specs or [VMEM] * len(args),
        out_specs=VMEM if one else tuple([VMEM] * len(shapes)),
        scratch_shapes=scratch,
        name=name,
    )(*args)


def shape(dims, dtype):
    return jax.ShapeDtypeStruct(dims, dtype)


def per_device(
    tokens,
    input_norm_gain,
    query_projection,
    key_projection,
    value_projection,
    write_strength_weight,
    decay_projection,
    head_decay_rate,
    token_extra_decay,
    accepted,
    prior_step_states,
    output_norm_gain,
    output_projection,
):
    def swap(x, axes):
        return lax.all_to_all(x, axes, 0, 0, tiled=True)

    packed = call(
        pack_kernel,
        shape((8, 32, WIDE), bf16),
        (
            jnp.transpose(tokens, (1, 2, 0)),
            input_norm_gain[None, :],
            query_projection,
            key_projection,
            value_projection,
            write_strength_weight.T,
            decay_projection.T,
            output_projection.T,
        ),
        name="pack",
    )
    near = swap(packed, NEAR)
    part = call(project_kernel, shape((64, SMALL + 128 - QKV), bf16), (near,), name="project")
    arrived = swap(part.reshape(8, 8, part.shape[1]), "z8").reshape(part.shape)
    states, rows = call(
        delta_kernel,
        (shape(prior_step_states.shape, f32), shape((64, 512), bf16)),
        (
            accepted,
            arrived,
            prior_step_states,
            head_decay_rate[None, :],
            token_extra_decay,
            output_norm_gain[None, :],
        ),
        specs=[SMEM] + [VMEM] * 5,
        scratch=[pltpu.VMEM((8, 128), f32), pltpu.VMEM((8, 512), f32)],
        name="delta",
    )
    all_rows = swap(rows.reshape(8, 8, 512), "z8").reshape(64, 512)
    columns = call(mix_kernel, shape((16, 32, 64), bf16), (near, all_rows), name="mix")
    back = swap(columns, ("zp", "y", "tp"))
    mixed = call(
        place_kernel, shape((4, 32, 128), bf16), (back, jnp.asarray(back_table())), name="place"
    )
    return (jnp.transpose(mixed, (2, 0, 1)), states)


def solution(mesh):
    split = Mesh(
        mesh.devices.reshape(mesh.shape["dp"], 8, 2, 4, mesh.shape["tp"]),
        ("dp", "z8", "zp", "y", "tp"),
    )
    in_specs = (
        P("dp", None, KV),
        P(KV),
        P(KV, "tp"),
        P(KV, "tp"),
        P(KV, "tp"),
        P(KV, "tp"),
        P(KV, "tp"),
        P("tp"),
        P(DP_KV, None, "tp"),
        P(DP_KV),
        P(DP_KV, None, "tp", None),
        P(),
        P("tp", KV),
    )
    out_specs = (P("dp", None, KV), P(DP_KV, None, "tp", None))
    return jax.shard_map(
        per_device, mesh=split, in_specs=in_specs, out_specs=out_specs, check_vma=False
    )
```

time: 181 us -> 99.6 us (0.55)
  waiting for transfers between devices: 37.2 us -> 0 us
  starting transfers between devices: 18.6 us -> 0 us
  Pallas kernels: 0 us -> 14.1 us
  blocking collectives: 95.4 us -> 82.5 us
  matrix products: 12.1 us -> 0 us
  local copies, waits for them, and re-layouts: 11.8 us -> 1.83 us
  other arithmetic: 4.17 us -> 0 us
    all_to_all x1 -> x0, waiting for transfers between devices: 37.2 us -> none  [sum_in_two_steps(): lax.all_to_all(nearer, far, split_axis=0, concat_axis=0, tiled=True)]
    all_gather x2 -> x0, blocking collectives: 36 us -> none  [gather_axes(): whole = lax.all_gather(whole, axes[number], axis=dim, tiled=True)]
    all_to_all x2 -> x4, blocking collectives: 59.4 us -> 82.5 us  [swap(): return lax.all_to_all(x, axes, 0, 0, tiled=True)]
    all_to_all x1 -> x0, starting transfers between devices: 18.6 us -> none  [sum_in_two_steps(): lax.all_to_all(nearer, far, split_axis=0, concat_axis=0, tiled=True)]
    pallas_call x0 -> x5, Pallas kernels: none -> 14.1 us  [call(): pl.pallas_call(kernel, out_shape=shapes, in_specs=specs or [VMEM] * len(a...]
    dot_general x12 -> x0, matrix products: 12.1 us -> none  [the longest x1 3.69 us: delta_block(): jnp.einsum('nhtj,nhjd,nhje->nhtde', within, key_heads, corrected, precisi...]
    concatenate x2 -> x0, local copies, waits for them, and re-layouts: 3.7 us -> none  [side_by_side(): both = jnp.concatenate(columns, axis=along)]
    reduce_sum x7 -> x0, other arithmetic: 2.36 us -> none  [the longest x1 1.16 us: summed_on_arrival(): return arrived.sum(axis=0)]
  transfers between devices with their start and end apart: 1 -> 0, of which waited for: 1 -> 0; matrix products, arithmetic and copies ran while one was open for 0% -> 0% of each run, Pallas kernels for 0% -> 0%
where the time goes in v1:
time: 99.6 us; the launch traced here: 99.1 us
  blocking collectives  82.5 us (83%)
  Pallas kernels  14.1 us (14%)
  local copies, waits for them, and re-layouts  1.83 us (2%)
    all_to_all x4, blocking collectives, swap(): return lax.all_to_all(x, axes, 0, 0, tiled=True)  82.5 us
    pallas_call x5, Pallas kernels, call(): pl.pallas_call(kernel, out_shape=shapes, in_specs=specs or [VMEM] * len(a...  14.1 us

profile of v1, /device:TPU:1, one launch (start us, length us, event | category | flops | bytes accessed | tf_op | source)
XLA Modules:
  0.0 99.1 jit_solution(14673723090254738059)
XLA Ops:
  0.6 2.3 %pack.1 = bf16[8,32,2304]{2,1,0:T(8,128)(2,1)} custom-call(bf16[4,32,128]{2,1,0:T(8,128)(2,1)} %bitcast.16, f32[1,32]{1,0:T(1,128)} %bitcast.21, bf16[32,512]{1,0:T(8,128)(2,1)} %q_ref.1, bf16[32,512]{1,0:T(8,128)(2,1)} %k_ref.1, bf16[32,512]{1,0:T(8,128)(2,1)} %v_ref.1, bf16[8,32]{1,0:T(8,128)(2,1)} %bitcast.19, bf16[8,32]{1,0:T(8,128)(2,1)} %bitcast.20, ...), custom_call_target="tpu_custom_call" | custom-call | tf_op jit(solution)/shard_map/pack/pallas_call | solution.py:184
  2.9 18.7 %all_to_all.20.x_ref = bf16[8,32,2304]{2,1,0:T(8,128)(2,1)} all-to-all(bf16[8,32,2304]{2,1,0:T(8,128)(2,1)} %pack.1), channel_id=1, replica_groups=mesh['dp'=4,'z8'=8,'zp'=2,'y'=4,'tp'=2] {'zp','y'}, dimensions={0} | all-to-all | bytes 2359296 | tf_op jit(solution)/shard_map/all_to_all | solution.py:214
  21.6 2.3 %project.1 = bf16[64,1664]{1,0:T(8,128)(2,1)} custom-call(bf16[8,32,2304]{2,1,0:T(8,128)(2,1)} %all_to_all.20.x_ref), custom_call_target="tpu_custom_call" | custom-call | tf_op jit(solution)/shard_map/project/pallas_call | solution.py:184
  23.9 34.3 %all_to_all.21 = bf16[8,8,1664]{2,1,0:T(8,128)(2,1)} all-to-all(bf16[8,8,1664]{2,1,0:T(8,128)(2,1)} %bitcast.13), channel_id=1, replica_groups=mesh['dp'=4,'z8'=8,'zp'=2,'y'=4,'tp'=2] {'z8'}, dimensions={0} | all-to-all | bytes 425984 | tf_op jit(solution)/shard_map/all_to_all | solution.py:214
  58.2 5.4 %delta.1 = (f32[2,4,8,4096]{3,2,1,0:T(8,128)}, bf16[64,512]{1,0:T(8,128)(2,1)}) custom-call(s32[2]{0:T(128)} %accepted_ref.1, bf16[64,1664]{1,0:T(8,128)(2,1)} %bitcast.12, f32[2,4,8,4096]{3,2,1,0:T(8,128)} %prior_ref.1, f32[1,8]{1,0:T(1,128)} %bitcast.22, f32[2,4,8]{2,1,0:T(4,128)} %extra_ref.1, f32[1,64]{1,0:T(1,128)} %bitcast.23), custom_call_target="tpu_custom_call" | custom-call | tf_op jit(solution)/shard_map/delta/pallas_call | solution.py:184
  63.6 16.7 %all_to_all.22 = bf16[8,8,512]{2,1,0:T(8,128)(2,1)} all-to-all(bf16[8,8,512]{2,1,0:T(8,128)(2,1)} %bitcast.15), channel_id=1, replica_groups=mesh['dp'=4,'z8'=8,'zp'=2,'y'=4,'tp'=2] {'z8'}, dimensions={0} | all-to-all | bytes 131072 | tf_op jit(solution)/shard_map/all_to_all | solution.py:214
  80.3 2.1 %mix.1 = bf16[16,32,64]{2,1,0:T(8,128)(2,1)} custom-call(bf16[8,32,2304]{2,1,0:T(8,128)(2,1)} %all_to_all.20.x_ref, bf16[64,512]{1,0:T(8,128)(2,1)} %bitcast.14), custom_call_target="tpu_custom_call" | custom-call | tf_op jit(solution)/shard_map/mix/pallas_call | solution.py:184
  82.5 1.0 %reshape.20 = bf16[16,2,1024]{2,1,0:T(2,128)(2,1)S(1)} reshape(bf16[16,32,64]{2,1,0:T(8,128)(2,1)} %mix.1) | data formatting | bytes 131072
  83.5 12.8 %all_to_all.23 = bf16[16,2,1024]{2,1,0:T(2,128)(2,1)S(1)} all-to-all(bf16[16,2,1024]{2,1,0:T(2,128)(2,1)S(1)} %reshape.20), channel_id=1, replica_groups=mesh['dp'=4,'z8'=8,'zp'=2,'y'=4,'tp'=2] {'zp','y','tp'}, dimensions={0} | all-to-all | bytes 131072 | tf_op jit(solution)/shard_map/all_to_all | solution.py:214
  96.3 0.8 reshape.21.x_ref
  97.1 1.9 %place.1 = bf16[4,32,128]{2,1,0:T(8,128)(2,1)} custom-call(bf16[16,32,64]{2,1,0:T(8,128)(2,1)} %reshape.21.x_ref, bf16[512,512]{1,0:T(8,128)(2,1)} %constant.2.clone.back_ref), custom_call_target="tpu_custom_call" | custom-call | tf_op jit(solution)/shard_map/place/pallas_call | solution.py:184

commit v2 on v1

--- a/solution.py
+++ b/solution.py
@@ -79,7 +79,8 @@
 
 
 def delta_kernel(
-    accepted_ref, c_ref, prior_ref, rate_ref, extra_ref, gain_ref, states_ref, rows_ref, aux, nrows
+    accepted_ref, c_ref, prior_ref, rate_ref, extra_ref, gain_ref, out_ref, rows_ref,
+    aux, nrows, states_ref, sems
 ):
     c = c_ref[...].astype(f32)
     s = c[0:8]
@@ -120,6 +121,7 @@
     def spread(values, i):
         return jnp.take_along_axis(values, lane // 64 + 2 * i, axis=1, mode="promise_in_bounds")
 
+    copies = []
     for j in range(2):
         start = accepted_ref[j] - 1
         state = [prior_ref[j, start, :, 128 * i : 128 * i + 128] for i in range(32)]
@@ -143,6 +145,10 @@
                 states_ref[j, t, :, 128 * i : 128 * i + 128] = state[i]
                 term = spread(q, i) * state[i]
                 sums[i % 4] = term if i < 4 else sums[i % 4] + term
+            copies.append(
+                pltpu.make_async_copy(states_ref.at[j, t], out_ref.at[j, t], sems.at[row])
+            )
+            copies[-1].start()
             o = (sums[0] + sums[1]) + (sums[2] + sums[3])
             o = o + pltpu.roll(o, 64, 1)
             mean = jnp.sum(o * o, axis=1, keepdims=True) / 128
@@ -153,23 +159,33 @@
                 )
     rows = nrows[...]
     rows_ref[...] = jnp.concatenate([rows] * 8, axis=0).astype(bf16)
+    for copy in copies:
+        copy.wait()
 
 
 def mix_kernel(x_ref, rows_ref, out_ref):
     w = x_ref[:, :, WO:QKV].reshape(256, 512)
-    out = dot(w, rows_ref[...], 1, 1).astype(bf16)
+    rows = rows_ref[...]
+    out = dot(w, jnp.concatenate([rows, rows], axis=0), 1, 1)
+    low = iota((16, 128), 1) < 64
     for r in range(8):
-        out_ref[2 * r] = out[32 * r : 32 * r + 32]
-        out_ref[2 * r + 1] = out[32 * r : 32 * r + 32]
+        piece = jnp.where(low, out[32 * r : 32 * r + 16], out[32 * r + 16 : 32 * r + 32])
+        out_ref[2 * r] = piece.astype(bf16)
+        out_ref[2 * r + 1] = piece.astype(bf16)
 
 
 def place_kernel(x_ref, back_ref, out_ref):
-    whole = jnp.zeros((32, 512), f32)
-    for r in range(8):
-        both = (x_ref[2 * r].astype(f32) + x_ref[2 * r + 1].astype(f32)).astype(bf16)
-        whole = whole + dot(both, back_ref[64 * r : 64 * r + 64, :], 1, 0)
+    low = iota((16, 128), 1) < 64
+    sums = [x_ref[2 * r].astype(f32) + x_ref[2 * r + 1].astype(f32) for r in range(8)]
+    tiles = []
+    for p in range(4):
+        a, b = sums[2 * p], sums[2 * p + 1]
+        top = jnp.where(low, a, pltpu.roll(b, 64, 1))
+        end = jnp.where(low, pltpu.roll(a, 64, 1), b)
+        tiles.append(jnp.concatenate([top, end], axis=0).astype(bf16))
+    whole = dot(jnp.concatenate(tiles, axis=1), back_ref[...], 1, 0).astype(bf16)
     for t in range(4):
-        out_ref[t] = whole[:, 128 * t : 128 * t + 128].astype(bf16)
+        out_ref[t] = whole[:, 128 * t : 128 * t + 128]
 
 
 def back_table():
@@ -179,14 +195,16 @@
     return (wanted[:, None] == np.arange(512)[None, :]).astype(jnp.bfloat16)
 
 
-def call(kernel, shapes, args, specs=None, scratch=(), name=None):
-    one = not isinstance(shapes, tuple)
+def call(kernel, shapes, args, specs=None, scratch=(), outs=VMEM, name=None):
+    if name == "pack":
+        args = [pltpu.with_memory_space_constraint(a, pltpu.HBM) for a in args]
     return pl.pallas_call(
         kernel,
         out_shape=shapes,
         in_specs=specs or [VMEM] * len(args),
-        out_specs=VMEM if one else tuple([VMEM] * len(shapes)),
+        out_specs=outs,
         scratch_shapes=scratch,
+        compiler_params=pltpu.CompilerParams(vmem_limit_bytes=16 << 20),
         name=name,
     )(*args)
 
@@ -243,11 +261,17 @@
             output_norm_gain[None, :],
         ),
         specs=[SMEM] + [VMEM] * 5,
-        scratch=[pltpu.VMEM((8, 128), f32), pltpu.VMEM((8, 512), f32)],
+        scratch=[
+            pltpu.VMEM((8, 128), f32),
+            pltpu.VMEM((8, 512), f32),
+            pltpu.VMEM((2, 4, 8, 4096), f32),
+            pltpu.SemaphoreType.DMA((8,)),
+        ],
+        outs=(pl.BlockSpec(memory_space=pltpu.HBM), VMEM),
         name="delta",
     )
     all_rows = swap(rows.reshape(8, 8, 512), "z8").reshape(64, 512)
-    columns = call(mix_kernel, shape((16, 32, 64), bf16), (near, all_rows), name="mix")
+    columns = call(mix_kernel, shape((16, 16, 128), bf16), (near, all_rows), name="mix")
     back = swap(columns, ("zp", "y", "tp"))
     mixed = call(
         place_kernel, shape((4, 32, 128), bf16), (back, jnp.asarray(back_table())), name="place"

time: 99.6 us -> 89.2 us (0.90)
  Pallas kernels: 14.1 us -> 7.18 us
  local copies, waits for them, and re-layouts: 1.83 us -> 0.03 us
  blocking collectives: 82.5 us -> 80.9 us
    pallas_call x5, Pallas kernels: 14.1 us -> 7.18 us  [call(): pl.pallas_call(kernel, out_shape=shapes, in_specs=specs or [VMEM] * len(a...]
    unnamed x2 -> x12, local copies, waits for them, and re-layouts: 1.83 us -> 0.03 us
    all_to_all x4, blocking collectives: 82.5 us -> 80.9 us  [swap(): return lax.all_to_all(x, axes, 0, 0, tiled=True)]
where the time goes in v2:
time: 89.2 us; the launch traced here: 88.8 us
  blocking collectives  80.9 us (91%)
  Pallas kernels  7.18 us (8%)
    all_to_all x4, blocking collectives, swap(): return lax.all_to_all(x, axes, 0, 0, tiled=True)  80.9 us
    pallas_call x5, Pallas kernels, call(): pl.pallas_call(kernel, out_shape=shapes, in_specs=specs or [VMEM] * len(a...  7.18 us

profile of v2, /device:TPU:1, one launch (start us, length us, event | category | flops | bytes accessed | tf_op | source)
XLA Modules:
  0.0 88.8 jit_solution(3376715335997803852)
XLA Ops:
  0.6 1.3 %pack.1 = bf16[8,32,2304]{2,1,0:T(8,128)(2,1)S(1)} custom-call(bf16[4,32,128]{2,1,0:T(8,128)(2,1)} %bitcast.18, f32[1,32]{1,0:T(1,128)} %bitcast.23, bf16[32,512]{1,0:T(8,128)(2,1)} %q_ref.1, bf16[32,512]{1,0:T(8,128)(2,1)} %k_ref.1, bf16[32,512]{1,0:T(8,128)(2,1)} %v_ref.1, bf16[8,32]{1,0:T(8,128)(2,1)} %bitcast.21, bf16[8,32]{1,0:T(8,128)(2,1)} %bitcast.22, ...), custom_call_target="tpu_custom_call" | custom-call | tf_op jit(solution)/shard_map/pack/pallas_call | solution.py:201
  2.0 19.8 %all_to_all.20.x_ref = bf16[8,32,2304]{2,1,0:T(8,128)(2,1)S(1)} all-to-all(bf16[8,32,2304]{2,1,0:T(8,128)(2,1)S(1)} %pack.1), channel_id=1, replica_groups=mesh['dp'=4,'z8'=8,'zp'=2,'y'=4,'tp'=2] {'zp','y'}, dimensions={0} | all-to-all | bytes 2359296 | tf_op jit(solution)/shard_map/all_to_all | solution.py:232
  21.7 0.0 copy-start
  21.7 0.0 copy-start.2
  21.7 0.0 copy-start.3
  21.7 0.0 copy-start.4
  21.7 0.0 copy-start.5
  21.7 0.4 project.1
  22.1 32.5 %all_to_all.21 = bf16[8,8,1664]{2,1,0:T(8,128)(2,1)S(1)} all-to-all(bf16[8,8,1664]{2,1,0:T(8,128)(2,1)S(1)} %bitcast.13), channel_id=1, replica_groups=mesh['dp'=4,'z8'=8,'zp'=2,'y'=4,'tp'=2] {'z8'}, dimensions={0} | all-to-all | bytes 425984 | tf_op jit(solution)/shard_map/all_to_all | solution.py:232
  54.7 0.0 copy-done
  54.7 0.0 copy-done.2
  54.7 0.0 copy-done.3
  54.7 0.0 copy-done.4
  54.7 0.0 copy-done.5
  54.7 0.0 copy-start.1
  54.7 4.4 %delta.1 = (f32[2,4,8,4096]{3,2,1,0:T(8,128)}, bf16[64,512]{1,0:T(8,128)(2,1)S(1)}) custom-call(s32[2]{0:T(128)S(1)} %copy-done.3, bf16[64,1664]{1,0:T(8,128)(2,1)S(1)} %bitcast.12, f32[2,4,8,4096]{3,2,1,0:T(8,128)S(1)} %copy-done, f32[1,8]{1,0:T(1,128)S(1)} %bitcast.16, f32[2,4,8]{2,1,0:T(4,128)S(1)} %copy-done.2, f32[1,64]{1,0:T(1,128)S(1)} %bitcast.17), custom_call_target="tpu_custom_call" | custom-call | tf_op jit(solution)/shard_map/delta/pallas_call | solution.py:201
  59.1 16.4 %all_to_all.22 = bf16[8,8,512]{2,1,0:T(8,128)(2,1)S(1)} all-to-all(bf16[8,8,512]{2,1,0:T(8,128)(2,1)S(1)} %bitcast.15), channel_id=1, replica_groups=mesh['dp'=4,'z8'=8,'zp'=2,'y'=4,'tp'=2] {'z8'}, dimensions={0} | all-to-all | bytes 131072 | tf_op jit(solution)/shard_map/all_to_all | solution.py:232
  75.6 0.2 mix.1
  75.8 12.2 %all_to_all.23.x_ref = bf16[16,16,128]{2,1,0:T(8,128)(2,1)S(1)} all-to-all(bf16[16,16,128]{2,1,0:T(8,128)(2,1)S(1)} %mix.1), channel_id=1, replica_groups=mesh['dp'=4,'z8'=8,'zp'=2,'y'=4,'tp'=2] {'zp','y','tp'}, dimensions={0} | all-to-all | bytes 131072 | tf_op jit(solution)/shard_map/all_to_all | solution.py:232
  88.0 0.0 copy-done.1
  88.0 0.9 place.1
Async XLA Ops:
  21.7 32.9 %copy-start = (f32[2,4,8,4096]{3,2,1,0:T(8,128)S(1)}, f32[2,4,8,4096]{3,2,1,0:T(8,128)}, u32[]{:S(2)}) copy-start(f32[2,4,8,4096]{3,2,1,0:T(8,128)} %prior_ref.1) | copy-start | bytes 3145732
  21.7 32.9 %copy-start.2 = (f32[2,4,8]{2,1,0:T(4,128)S(1)}, f32[2,4,8]{2,1,0:T(4,128)}, u32[]{:S(2)}) copy-start(f32[2,4,8]{2,1,0:T(4,128)} %extra_ref.1) | copy-start | bytes 772
  21.7 32.9 %copy-start.3 = (s32[2]{0:T(128)S(1)}, s32[2]{0:T(128)}, u32[]{:S(2)}) copy-start(s32[2]{0:T(128)} %accepted_ref.1) | copy-start | bytes 28
  21.7 32.9 %copy-start.4 = (f32[8]{0:T(128)S(1)}, f32[8]{0:T(128)}, u32[]{:S(2)}) copy-start(f32[8]{0:T(128)} %param.21) | copy-start | bytes 100
  21.7 32.9 %copy-start.5 = (f32[64]{0:T(128)S(1)}, f32[64]{0:T(128)}, u32[]{:S(2)}) copy-start(f32[64]{0:T(128)} %param.25) | copy-start | bytes 772
  54.7 33.3 %copy-start.1 = (bf16[512,512]{1,0:T(8,128)(2,1)S(1)}, bf16[512,512]{1,0:T(8,128)(2,1)}, u32[]{:S(2)}) copy-start(bf16[512,512]{1,0:T(8,128)(2,1)} %constant.2.clone.back_ref) | copy-start | bytes 1572868

commit v3 on v2

--- a/solution.py
+++ b/solution.py
@@ -15,9 +15,10 @@
 f32 = jnp.float32
 bf16 = jnp.bfloat16
 
-WO, QKV, SMALL, TOK, WIDE = 0, 512, 2048, 2176, 2304
+WO, QKV, SMALL, WIDE = 0, 512, 2048, 2176
 VMEM = pl.BlockSpec(memory_space=pltpu.VMEM)
 SMEM = pl.BlockSpec(memory_space=pltpu.SMEM)
+HBM = pl.BlockSpec(memory_space=pltpu.HBM)
 
 
 def iota(shape, dim):
@@ -28,64 +29,86 @@
     return lax.dot_general(a, b, (((ca,), (cb,)), ((), ())), preferred_element_type=f32)
 
 
-def pack_kernel(tok_ref, gain_ref, q_ref, k_ref, v_ref, beta_ref, decay_ref, wo_ref, out_ref):
-    eye = iota((32, 32), 0) == iota((32, 32), 1)
-    gain = jnp.sum(jnp.where(eye, gain_ref[...], 0.0), axis=1, keepdims=True)
-    raw = jnp.concatenate([tok_ref[t] for t in range(4)], axis=1)
-    scaled = (raw.astype(f32) * gain).astype(bf16)
-    source, dest = iota((512, 512), 0), iota((512, 512), 1)
+def pack_kernel(*refs):
+    hbm, out_ref, held, sems = refs[:8], refs[8], refs[9:17], refs[17]
+    copies = [pltpu.make_async_copy(hbm[n], held[n], sems.at[n]) for n in range(8)]
+    for copy in copies:
+        copy.start()
+    tok_ref, gain_ref, q_ref, k_ref, v_ref, beta_ref, decay_ref, wo_ref = held
+    source, dest = iota((512, 512), 0), iota((1, 512), 1)
     group, rho = dest // 64, dest % 64
     wanted = (rho % 4) * 128 + (rho // 8) * 16 + group * 2 + (rho % 8) // 4
     pick = (source == wanted).astype(f32).astype(bf16)
-    both = dot(jnp.concatenate([scaled, raw], axis=0), pick, 1, 0)
+    eye = iota((32, 32), 0) == iota((32, 32), 1)
     head, lane = iota((8, 128), 0), iota((8, 128), 1)
     put_beta = ((lane == head) | (lane == head + 16)).astype(f32).astype(bf16)
     put_decay = ((lane == head + 8) | (lane == head + 24)).astype(f32).astype(bf16)
+    copies[0].wait()
+    copies[1].wait()
+    gain = jnp.sum(jnp.where(eye, gain_ref[...], 0.0), axis=1, keepdims=True)
+    raw = jnp.concatenate([tok_ref[t] for t in range(4)], axis=1).astype(f32)
+    scaled = raw * gain
+    squares = jnp.sum(raw * raw, axis=0, keepdims=True)
+    high = squares.astype(bf16).astype(f32)
+    sub = iota((16, 512), 0)
+    extra = jnp.where(sub < 2, high, jnp.where(sub < 4, squares - high, 0.0))
+    moved = dot(jnp.concatenate([scaled, extra], axis=0).astype(bf16), pick, 1, 0)
+    copies[5].wait()
+    copies[6].wait()
     small = dot(beta_ref[...], put_beta, 0, 0) + dot(decay_ref[...], put_decay, 0, 0)
-    small = small.astype(bf16)
-    low = iota((32, 128), 1) < 64
+    lane = iota((8, 128), 1)
+    even = iota((8, 128), 0) % 2 == 0
+    for n in (2, 3, 4, 7):
+        copies[n].wait()
     for r in range(8):
-        s = both[:32, 128 * (r // 2) : 128 * (r // 2) + 128]
-        w = both[32:, 128 * (r // 2) : 128 * (r // 2) + 128]
+        at = slice(128 * (r // 2), 128 * (r // 2) + 128)
+        sums = moved[32:40, at]
         if r % 2 == 0:
-            tile = jnp.where(low, s, pltpu.roll(w, 64, 1))
+            cols = pltpu.roll(moved[:32, at], 64, 1)
+            sums = jnp.where(even, pltpu.roll(sums, 32, 1), sums)
         else:
-            tile = jnp.where(low, pltpu.roll(s, 64, 1), w)
+            cols = moved[:32, at]
+            sums = jnp.where(even, pltpu.roll(sums, 96, 1), pltpu.roll(sums, 64, 1))
+        groups = []
+        for g in range(4):
+            right = jnp.where(lane < 64, sums if g == 0 else 0.0, cols[8 * g : 8 * g + 8])
+            groups.append(jnp.where(lane < 32, small[8 * g : 8 * g + 8], right))
+        tile = jnp.concatenate(groups, axis=0)
         out_ref[r, :, WO:QKV] = wo_ref[...]
         out_ref[r, :, QKV : QKV + 512] = q_ref[...]
         out_ref[r, :, QKV + 512 : QKV + 1024] = k_ref[...]
         out_ref[r, :, QKV + 1024 : SMALL] = v_ref[...]
-        out_ref[r, :, SMALL:TOK] = small
-        out_ref[r, :, TOK:] = tile.astype(bf16)
+        out_ref[r, :, SMALL:] = tile.astype(bf16)
 
 
 def project_kernel(x_ref, out_ref):
     x = x_ref[...].reshape(256, WIDE)
-    cols = x[:, TOK:]
-    raw = cols.astype(f32)
-    square = raw * raw
-    high = square.astype(bf16)
-    rest = (square - high.astype(f32)).astype(bf16)
-    lane = iota((256, 128), 1)
-    ones = ((lane == 32) | (lane == 33)).astype(f32).astype(bf16)
-    sums = dot(high, ones, 0, 0) + dot(rest, ones, 0, 0)
+    cols = x[:, SMALL:]
     main = dot(cols, x[:, QKV:SMALL], 0, 0)
-    out_ref[:, : SMALL - QKV] = main[:64].astype(bf16)
-    tail = dot(cols, x[:, SMALL:TOK], 0, 0)[:64] + sums[64:]
+    out_ref[:, : SMALL - QKV] = main[64:].astype(bf16)
+    sums = jnp.zeros((8, 128), f32)
+    for r in range(8):
+        sums = sums + cols[32 * r : 32 * r + 16].astype(f32)[0:8]
+    sub, lane = iota((32, 128), 0), iota((32, 128), 1)
+    halves = []
+    for n in range(2):
+        row = sums[n : n + 1] + sums[n + 2 : n + 3]
+        halves.append(jnp.sum(jnp.where(lane == sub + 32, row, 0.0), axis=1, keepdims=True))
+    total = jnp.concatenate(halves, axis=0)
+    lane = iota((64, 128), 1)
+    tail = jnp.where(lane < 32, dot(cols, cols, 0, 0)[64:], jnp.where(lane < 34, total, 0.0))
     first = tail.astype(bf16).astype(f32)
-    lane = iota((64, 128), 1)
     keep = (lane < 16) | (lane == 32)
     out_ref[:, SMALL - QKV :] = jnp.where(keep, first, tail - first).astype(bf16)
 
 
 def delta_kernel(
     accepted_ref, c_ref, prior_ref, rate_ref, extra_ref, gain_ref, out_ref, rows_ref,
-    aux, nrows, states_ref, sems
+    aux, nrows, states_ref, kept, sems
 ):
     c = c_ref[...].astype(f32)
-    s = c[0:8]
-    for z in range(1, 8):
-        s = s + c[8 * z : 8 * z + 8]
+    s = (c[0:8] + c[8:16]) + (c[16:24] + c[24:32])
+    s = s + ((c[32:40] + c[40:48]) + (c[48:56] + c[56:64]))
     tile = s[:, 1536:]
     total = tile[:, 32:33] + tile[:, 33:34]
     inverse = lax.rsqrt(total / D + epsilon)
@@ -115,48 +138,79 @@
             m = jnp.where(masks[p], piece, m)
         return m + pltpu.roll(m, 64, 1)
 
+    def half_sum(values):
+        return 0.5 * jnp.sum(values, axis=1, keepdims=True)
+
     def unit(values):
-        return values * lax.rsqrt(0.5 * jnp.sum(values * values, axis=1, keepdims=True) + epsilon)
-
-    def spread(values, i):
-        return jnp.take_along_axis(values, lane // 64 + 2 * i, axis=1, mode="promise_in_bounds")
+        return values * lax.rsqrt(half_sum(values * values) + epsilon)
+
+    ROWS = range(8)
+    q = [unit(by_heads(parts[0], row)) * 0.125 for row in ROWS]
+    k = [unit(by_heads(parts[1], row)) for row in ROWS]
+    v = [by_heads(parts[2], row) for row in ROWS]
+    a = [jnp.broadcast_to(fade[:, row : row + 1], (8, 128)) for row in ROWS]
+    b = [jnp.broadcast_to(beta[:, row : row + 1], (8, 128)) for row in ROWS]
+
+    starts = [accepted_ref[0] - 1, accepted_ref[1] - 1]
+    ks, qs = [None] * 8, [None] * 8
+    for i in range(32):
+        index = lane // 64 + 2 * i
+        at = slice(128 * i, 128 * i + 128)
+        for j in range(2):
+            start = prior_ref[j, starts[j], :, at]
+            for row in range(4 * j, 4 * j + 4):
+                kx = jnp.take_along_axis(k[row], index, axis=1, mode="promise_in_bounds")
+                qx = jnp.take_along_axis(q[row], index, axis=1, mode="promise_in_bounds")
+                kept[row, :, at] = kx
+                ks[row] = kx * start if i == 0 else ks[row] + kx * start
+                qs[row] = qx * start if i == 0 else qs[row] + qx * start
+
+    def fold(values):
+        return values + pltpu.roll(values, 64, 1)
+
+    ks = [fold(values) for values in ks]
+    qs = [fold(values) for values in qs]
+    w, o = [None] * 8, [None] * 8
+    for j in range(2):
+        base = 4 * j
+        grown = None
+        for t in range(4):
+            row = base + t
+            carried = ks[row] if t == 0 else grown * ks[row]
+            for e in range(t):
+                reach = half_sum(k[row] * k[base + e])
+                for m in range(e + 1, t):
+                    reach = reach * a[base + m]
+                carried = carried + reach * w[base + e]
+            w[row] = b[row] * (v[row] - a[row] * carried)
+            grown = a[row] if t == 0 else grown * a[row]
+            out = grown * qs[row] + half_sum(q[row] * k[row]) * w[row]
+            for e in range(t):
+                reach = half_sum(q[row] * k[base + e])
+                for m in range(e + 1, t + 1):
+                    reach = reach * a[base + m]
+                out = out + reach * w[base + e]
+            o[row] = out
 
     copies = []
     for j in range(2):
-        start = accepted_ref[j] - 1
-        state = [prior_ref[j, start, :, 128 * i : 128 * i + 128] for i in range(32)]
-        for t in range(4):
-            row = 4 * j + t
-            q = unit(by_heads(parts[0], row)) * 0.125
-            k = unit(by_heads(parts[1], row))
-            v = by_heads(parts[2], row)
-            a = jnp.broadcast_to(fade[:, row : row + 1], (8, 128))
-            b = jnp.broadcast_to(beta[:, row : row + 1], (8, 128))
-            kx = [spread(k, i) for i in range(32)]
-            sums = [kx[i] * state[i] for i in range(4)]
-            for i in range(4, 32):
-                sums[i % 4] = sums[i % 4] + kx[i] * state[i]
-            u = (sums[0] + sums[1]) + (sums[2] + sums[3])
-            u = u + pltpu.roll(u, 64, 1)
-            w = b * (v - a * u)
-            sums = [None] * 4
-            for i in range(32):
-                state[i] = a * state[i] + kx[i] * w
-                states_ref[j, t, :, 128 * i : 128 * i + 128] = state[i]
-                term = spread(q, i) * state[i]
-                sums[i % 4] = term if i < 4 else sums[i % 4] + term
-            copies.append(
-                pltpu.make_async_copy(states_ref.at[j, t], out_ref.at[j, t], sems.at[row])
+        for i in range(32):
+            at = slice(128 * i, 128 * i + 128)
+            state = prior_ref[j, starts[j], :, at]
+            for t in range(4):
+                row = 4 * j + t
+                state = a[row] * state + kept[row, :, at] * w[row]
+                states_ref[j, t, :, at] = state
+        copies.append(pltpu.make_async_copy(states_ref.at[j], out_ref.at[j], sems.at[j]))
+        copies[-1].start()
+
+    for row in ROWS:
+        mean = half_sum(o[row] * o[row]) / 64
+        n = o[row] * lax.rsqrt(mean + epsilon) * gain
+        for p in range(4):
+            nrows[row : row + 1, 128 * p : 128 * p + 128] = jnp.sum(
+                jnp.where(masks[p], n, 0.0), axis=0, keepdims=True
             )
-            copies[-1].start()
-            o = (sums[0] + sums[1]) + (sums[2] + sums[3])
-            o = o + pltpu.roll(o, 64, 1)
-            mean = jnp.sum(o * o, axis=1, keepdims=True) / 128
-            n = o * lax.rsqrt(mean + epsilon) * gain
-            for p in range(4):
-                nrows[row : row + 1, 128 * p : 128 * p + 128] = jnp.sum(
-                    jnp.where(masks[p], n, 0.0), axis=0, keepdims=True
-                )
     rows = nrows[...]
     rows_ref[...] = jnp.concatenate([rows] * 8, axis=0).astype(bf16)
     for copy in copies:
@@ -244,10 +298,22 @@
             decay_projection.T,
             output_projection.T,
         ),
+        specs=[HBM] * 8,
+        scratch=[
+            pltpu.VMEM((4, 32, 128), bf16),
+            pltpu.VMEM((1, 32), f32),
+            pltpu.VMEM((32, 512), bf16),
+            pltpu.VMEM((32, 512), bf16),
+            pltpu.VMEM((32, 512), bf16),
+            pltpu.VMEM((8, 32), bf16),
+            pltpu.VMEM((8, 32), bf16),
+            pltpu.VMEM((32, 512), bf16),
+            pltpu.SemaphoreType.DMA((8,)),
+        ],
         name="pack",
     )
     near = swap(packed, NEAR)
-    part = call(project_kernel, shape((64, SMALL + 128 - QKV), bf16), (near,), name="project")
+    part = call(project_kernel, shape((64, WIDE - QKV), bf16), (near,), name="project")
     arrived = swap(part.reshape(8, 8, part.shape[1]), "z8").reshape(part.shape)
     states, rows = call(
         delta_kernel,
@@ -265,9 +331,10 @@
             pltpu.VMEM((8, 128), f32),
             pltpu.VMEM((8, 512), f32),
             pltpu.VMEM((2, 4, 8, 4096), f32),
-            pltpu.SemaphoreType.DMA((8,)),
+            pltpu.VMEM((8, 8, 4096), f32),
+            pltpu.SemaphoreType.DMA((2,)),
         ],
-        outs=(pl.BlockSpec(memory_space=pltpu.HBM), VMEM),
+        outs=(HBM, VMEM),
         name="delta",
     )
     all_rows = swap(rows.reshape(8, 8, 512), "z8").reshape(64, 512)

time: 89.2 us -> 87.3 us (0.979)
  Pallas kernels: 7.18 us -> 5.64 us
    pallas_call x5, Pallas kernels: 7.18 us -> 5.64 us  [call(): pl.pallas_call(kernel, out_shape=shapes, in_specs=specs or [VMEM] * len(a...]
where the time goes in v3:
time: 87.3 us; the launch traced here: 87 us
  blocking collectives  80.6 us (92%)
  Pallas kernels  5.64 us (6%)
    all_to_all x4, blocking collectives, swap(): return lax.all_to_all(x, axes, 0, 0, tiled=True)  80.6 us
    pallas_call x5, Pallas kernels, call(): pl.pallas_call(kernel, out_shape=shapes, in_specs=specs or [VMEM] * len(a...  5.64 us

profile of v3, /device:TPU:1, one launch (start us, length us, event | category | flops | bytes accessed | tf_op | source)
XLA Modules:
  0.0 87.0 jit_solution(1262442083623425887)
XLA Ops:
  0.6 1.4 %pack.1 = bf16[8,32,2176]{2,1,0:T(8,128)(2,1)S(1)} custom-call(bf16[4,32,128]{2,1,0:T(8,128)(2,1)} %bitcast.18, f32[1,32]{1,0:T(1,128)} %bitcast.23, bf16[32,512]{1,0:T(8,128)(2,1)} %refs_2_.1, bf16[32,512]{1,0:T(8,128)(2,1)} %refs_3_.1, bf16[32,512]{1,0:T(8,128)(2,1)} %refs_4_.1, bf16[8,32]{1,0:T(8,128)(2,1)} %bitcast.21, bf16[8,32]{1,0:T(8,128)(2,1)} %bitcast.22, ...), custom_call_target="tpu_custom_call" | custom-call | tf_op jit(solution)/shard_map/pack/pallas_call | solution.py:255
  2.0 19.4 %all_to_all.20.x_ref = bf16[8,32,2176]{2,1,0:T(8,128)(2,1)S(1)} all-to-all(bf16[8,32,2176]{2,1,0:T(8,128)(2,1)S(1)} %pack.1), channel_id=1, replica_groups=mesh['dp'=4,'z8'=8,'zp'=2,'y'=4,'tp'=2] {'zp','y'}, dimensions={0} | all-to-all | bytes 2228224 | tf_op jit(solution)/shard_map/all_to_all | solution.py:286
  21.4 0.0 copy-start
  21.4 0.0 copy-start.2
  21.4 0.0 copy-start.3
  21.4 0.0 copy-start.4
  21.4 0.0 copy-start.5
  21.4 0.3 project.1
  21.7 32.6 %all_to_all.21 = bf16[8,8,1664]{2,1,0:T(8,128)(2,1)S(1)} all-to-all(bf16[8,8,1664]{2,1,0:T(8,128)(2,1)S(1)} %bitcast.13), channel_id=1, replica_groups=mesh['dp'=4,'z8'=8,'zp'=2,'y'=4,'tp'=2] {'z8'}, dimensions={0} | all-to-all | bytes 425984 | tf_op jit(solution)/shard_map/all_to_all | solution.py:286
  54.3 0.0 copy-done
  54.3 0.0 copy-done.2
  54.3 0.0 copy-done.3
  54.3 0.0 copy-done.4
  54.4 0.0 copy-done.5
  54.4 0.0 copy-start.1
  54.4 2.9 %delta.1 = (f32[2,4,8,4096]{3,2,1,0:T(8,128)}, bf16[64,512]{1,0:T(8,128)(2,1)S(1)}) custom-call(s32[2]{0:T(128)S(1)} %copy-done.3, bf16[64,1664]{1,0:T(8,128)(2,1)S(1)} %bitcast.12, f32[2,4,8,4096]{3,2,1,0:T(8,128)S(1)} %copy-done, f32[1,8]{1,0:T(1,128)S(1)} %bitcast.16, f32[2,4,8]{2,1,0:T(4,128)S(1)} %copy-done.2, f32[1,64]{1,0:T(1,128)S(1)} %bitcast.17), custom_call_target="tpu_custom_call" | custom-call | tf_op jit(solution)/shard_map/delta/pallas_call | solution.py:255
  57.3 16.7 %all_to_all.22 = bf16[8,8,512]{2,1,0:T(8,128)(2,1)S(1)} all-to-all(bf16[8,8,512]{2,1,0:T(8,128)(2,1)S(1)} %bitcast.15), channel_id=1, replica_groups=mesh['dp'=4,'z8'=8,'zp'=2,'y'=4,'tp'=2] {'z8'}, dimensions={0} | all-to-all | bytes 131072 | tf_op jit(solution)/shard_map/all_to_all | solution.py:286
  73.9 0.2 mix.1
  74.1 12.0 %all_to_all.23.x_ref = bf16[16,16,128]{2,1,0:T(8,128)(2,1)S(1)} all-to-all(bf16[16,16,128]{2,1,0:T(8,128)(2,1)S(1)} %mix.1), channel_id=1, replica_groups=mesh['dp'=4,'z8'=8,'zp'=2,'y'=4,'tp'=2] {'zp','y','tp'}, dimensions={0} | all-to-all | bytes 131072 | tf_op jit(solution)/shard_map/all_to_all | solution.py:286
  86.1 0.0 copy-done.1
  86.2 0.9 place.1
Async XLA Ops:
  21.4 32.9 %copy-start = (f32[2,4,8,4096]{3,2,1,0:T(8,128)S(1)}, f32[2,4,8,4096]{3,2,1,0:T(8,128)}, u32[]{:S(2)}) copy-start(f32[2,4,8,4096]{3,2,1,0:T(8,128)} %prior_ref.1) | copy-start | bytes 3145732
  21.4 32.9 %copy-start.2 = (f32[2,4,8]{2,1,0:T(4,128)S(1)}, f32[2,4,8]{2,1,0:T(4,128)}, u32[]{:S(2)}) copy-start(f32[2,4,8]{2,1,0:T(4,128)} %extra_ref.1) | copy-start | bytes 772
  21.4 32.9 %copy-start.3 = (s32[2]{0:T(128)S(1)}, s32[2]{0:T(128)}, u32[]{:S(2)}) copy-start(s32[2]{0:T(128)} %accepted_ref.1) | copy-start | bytes 28
  21.4 32.9 %copy-start.4 = (f32[8]{0:T(128)S(1)}, f32[8]{0:T(128)}, u32[]{:S(2)}) copy-start(f32[8]{0:T(128)} %param.21) | copy-start | bytes 100
  21.4 32.9 %copy-start.5 = (f32[64]{0:T(128)S(1)}, f32[64]{0:T(128)}, u32[]{:S(2)}) copy-start(f32[64]{0:T(128)} %param.25) | copy-start | bytes 772
  54.4 31.8 %copy-start.1 = (bf16[512,512]{1,0:T(8,128)(2,1)S(1)}, bf16[512,512]{1,0:T(8,128)(2,1)}, u32[]{:S(2)}) copy-start(bf16[512,512]{1,0:T(8,128)(2,1)} %constant.2.clone.back_ref) | copy-start | bytes 1572868

commit v4 on v3

--- a/solution.py
+++ b/solution.py
@@ -103,8 +103,8 @@
 
 
 def delta_kernel(
-    accepted_ref, c_ref, prior_ref, rate_ref, extra_ref, gain_ref, out_ref, rows_ref,
-    aux, nrows, states_ref, kept, sems
+    accepted_ref, c_ref, prior_ref, rate_ref, extra_ref, gain_ref, states_ref, rows_ref,
+    aux, nrows, kept
 ):
     c = c_ref[...].astype(f32)
     s = (c[0:8] + c[8:16]) + (c[16:24] + c[24:32])
@@ -192,7 +192,6 @@
                 out = out + reach * w[base + e]
             o[row] = out
 
-    copies = []
     for j in range(2):
         for i in range(32):
             at = slice(128 * i, 128 * i + 128)
@@ -201,8 +200,6 @@
                 row = 4 * j + t
                 state = a[row] * state + kept[row, :, at] * w[row]
                 states_ref[j, t, :, at] = state
-        copies.append(pltpu.make_async_copy(states_ref.at[j], out_ref.at[j], sems.at[j]))
-        copies[-1].start()
 
     for row in ROWS:
         mean = half_sum(o[row] * o[row]) / 64
@@ -213,8 +210,6 @@
             )
     rows = nrows[...]
     rows_ref[...] = jnp.concatenate([rows] * 8, axis=0).astype(bf16)
-    for copy in copies:
-        copy.wait()
 
 
 def mix_kernel(x_ref, rows_ref, out_ref):
@@ -228,7 +223,9 @@
         out_ref[2 * r + 1] = piece.astype(bf16)
 
 
-def place_kernel(x_ref, back_ref, out_ref):
+def place_kernel(x_ref, back_ref, states_ref, out_ref, kept_ref, sem):
+    copy = pltpu.make_async_copy(states_ref, kept_ref, sem)
+    copy.start()
     low = iota((16, 128), 1) < 64
     sums = [x_ref[2 * r].astype(f32) + x_ref[2 * r + 1].astype(f32) for r in range(8)]
     tiles = []
@@ -240,6 +237,7 @@
     whole = dot(jnp.concatenate(tiles, axis=1), back_ref[...], 1, 0).astype(bf16)
     for t in range(4):
         out_ref[t] = whole[:, 128 * t : 128 * t + 128]
+    copy.wait()
 
 
 def back_table():
@@ -330,20 +328,23 @@
         scratch=[
             pltpu.VMEM((8, 128), f32),
             pltpu.VMEM((8, 512), f32),
-            pltpu.VMEM((2, 4, 8, 4096), f32),
             pltpu.VMEM((8, 8, 4096), f32),
-            pltpu.SemaphoreType.DMA((2,)),
         ],
-        outs=(HBM, VMEM),
+        outs=(VMEM, VMEM),
         name="delta",
     )
     all_rows = swap(rows.reshape(8, 8, 512), "z8").reshape(64, 512)
     columns = call(mix_kernel, shape((16, 16, 128), bf16), (near, all_rows), name="mix")
     back = swap(columns, ("zp", "y", "tp"))
-    mixed = call(
-        place_kernel, shape((4, 32, 128), bf16), (back, jnp.asarray(back_table())), name="place"
-    )
-    return (jnp.transpose(mixed, (2, 0, 1)), states)
+    mixed, kept = call(
+        place_kernel,
+        (shape((4, 32, 128), bf16), shape(states.shape, f32)),
+        (back, jnp.asarray(back_table()), states),
+        scratch=[pltpu.SemaphoreType.DMA],
+        outs=(VMEM, HBM),
+        name="place",
+    )
+    return (jnp.transpose(mixed, (2, 0, 1)), kept)
 
 
 def solution(mesh):

time: 87.3 us -> 87.2 us (level)
  no operation moved by 1% of the time
where the time goes in v4:
time: 87.2 us; the launch traced here: 86.9 us
  blocking collectives  80.6 us (92%)
  Pallas kernels  5.53 us (6%)
    all_to_all x4, blocking collectives, swap(): return lax.all_to_all(x, axes, 0, 0, tiled=True)  80.6 us
    pallas_call x5, Pallas kernels, call(): pl.pallas_call(kernel, out_shape=shapes, in_specs=specs or [VMEM] * len(a...  5.53 us

profile of v4, /device:TPU:1, one launch (start us, length us, event | category | flops | bytes accessed | tf_op | source)
XLA Modules:
  0.0 86.9 jit_solution(14033455496549571243)
XLA Ops:
  0.6 1.4 %pack.1 = bf16[8,32,2176]{2,1,0:T(8,128)(2,1)S(1)} custom-call(bf16[4,32,128]{2,1,0:T(8,128)(2,1)} %bitcast.18, f32[1,32]{1,0:T(1,128)} %bitcast.22, bf16[32,512]{1,0:T(8,128)(2,1)} %refs_2_.1, bf16[32,512]{1,0:T(8,128)(2,1)} %refs_3_.1, bf16[32,512]{1,0:T(8,128)(2,1)} %refs_4_.1, bf16[8,32]{1,0:T(8,128)(2,1)} %bitcast.20, bf16[8,32]{1,0:T(8,128)(2,1)} %bitcast.21, ...), custom_call_target="tpu_custom_call" | custom-call | tf_op jit(solution)/shard_map/pack/pallas_call | solution.py:253
  2.0 19.4 %all_to_all.20.x_ref = bf16[8,32,2176]{2,1,0:T(8,128)(2,1)S(1)} all-to-all(bf16[8,32,2176]{2,1,0:T(8,128)(2,1)S(1)} %pack.1), channel_id=1, replica_groups=mesh['dp'=4,'z8'=8,'zp'=2,'y'=4,'tp'=2] {'zp','y'}, dimensions={0} | all-to-all | bytes 2228224 | tf_op jit(solution)/shard_map/all_to_all | solution.py:284
  21.4 0.0 copy-start
  21.4 0.0 copy-start.2
  21.4 0.0 copy-start.3
  21.4 0.0 copy-start.4
  21.4 0.0 copy-start.5
  21.4 0.3 project.1
  21.7 32.6 %all_to_all.21 = bf16[8,8,1664]{2,1,0:T(8,128)(2,1)S(1)} all-to-all(bf16[8,8,1664]{2,1,0:T(8,128)(2,1)S(1)} %bitcast.13), channel_id=1, replica_groups=mesh['dp'=4,'z8'=8,'zp'=2,'y'=4,'tp'=2] {'z8'}, dimensions={0} | all-to-all | bytes 425984 | tf_op jit(solution)/shard_map/all_to_all | solution.py:284
  54.3 0.0 copy-done
  54.3 0.0 copy-done.2
  54.3 0.0 copy-done.3
  54.3 0.0 copy-done.4
  54.4 0.0 copy-done.5
  54.4 0.0 copy-start.1
  54.4 2.0 %delta.1 = (f32[2,4,8,4096]{3,2,1,0:T(8,128)S(1)}, bf16[64,512]{1,0:T(8,128)(2,1)S(1)}) custom-call(s32[2]{0:T(128)S(1)} %copy-done.3, bf16[64,1664]{1,0:T(8,128)(2,1)S(1)} %bitcast.12, f32[2,4,8,4096]{3,2,1,0:T(8,128)S(1)} %copy-done, f32[1,8]{1,0:T(1,128)S(1)} %bitcast.16, f32[2,4,8]{2,1,0:T(4,128)S(1)} %copy-done.2, f32[1,64]{1,0:T(1,128)S(1)} %bitcast.17), custom_call_target="tpu_custom_call" | custom-call | tf_op jit(solution)/shard_map/delta/pallas_call | solution.py:253
  56.4 16.7 %all_to_all.22 = bf16[8,8,512]{2,1,0:T(8,128)(2,1)S(1)} all-to-all(bf16[8,8,512]{2,1,0:T(8,128)(2,1)S(1)} %bitcast.15), channel_id=1, replica_groups=mesh['dp'=4,'z8'=8,'zp'=2,'y'=4,'tp'=2] {'z8'}, dimensions={0} | all-to-all | bytes 131072 | tf_op jit(solution)/shard_map/all_to_all | solution.py:284
  73.0 0.2 mix.1
  73.3 12.0 %all_to_all.23.x_ref = bf16[16,16,128]{2,1,0:T(8,128)(2,1)S(1)} all-to-all(bf16[16,16,128]{2,1,0:T(8,128)(2,1)S(1)} %mix.1), channel_id=1, replica_groups=mesh['dp'=4,'z8'=8,'zp'=2,'y'=4,'tp'=2] {'zp','y','tp'}, dimensions={0} | all-to-all | bytes 131072 | tf_op jit(solution)/shard_map/all_to_all | solution.py:284
  85.3 0.0 copy-done.1
  85.3 1.6 %place.1 = (bf16[4,32,128]{2,1,0:T(8,128)(2,1)}, f32[2,4,8,4096]{3,2,1,0:T(8,128)}) custom-call(bf16[16,16,128]{2,1,0:T(8,128)(2,1)S(1)} %all_to_all.23.x_ref, bf16[512,512]{1,0:T(8,128)(2,1)S(1)} %copy-done.1, f32[2,4,8,4096]{3,2,1,0:T(8,128)S(1)} %get-tuple-element.7.states_ref), custom_call_target="tpu_custom_call" | custom-call | tf_op jit(solution)/shard_map/place/pallas_call | solution.py:253
Async XLA Ops:
  21.4 32.9 %copy-start = (f32[2,4,8,4096]{3,2,1,0:T(8,128)S(1)}, f32[2,4,8,4096]{3,2,1,0:T(8,128)}, u32[]{:S(2)}) copy-start(f32[2,4,8,4096]{3,2,1,0:T(8,128)} %prior_ref.1) | copy-start | bytes 3145732
  21.4 32.9 %copy-start.2 = (f32[2,4,8]{2,1,0:T(4,128)S(1)}, f32[2,4,8]{2,1,0:T(4,128)}, u32[]{:S(2)}) copy-start(f32[2,4,8]{2,1,0:T(4,128)} %extra_ref.1) | copy-start | bytes 772
  21.4 32.9 %copy-start.3 = (s32[2]{0:T(128)S(1)}, s32[2]{0:T(128)}, u32[]{:S(2)}) copy-start(s32[2]{0:T(128)} %accepted_ref.1) | copy-start | bytes 28
  21.4 32.9 %copy-start.4 = (f32[8]{0:T(128)S(1)}, f32[8]{0:T(128)}, u32[]{:S(2)}) copy-start(f32[8]{0:T(128)} %param.21) | copy-start | bytes 100
  21.4 32.9 %copy-start.5 = (f32[64]{0:T(128)S(1)}, f32[64]{0:T(128)}, u32[]{:S(2)}) copy-start(f32[64]{0:T(128)} %param.25) | copy-start | bytes 772
  54.4 30.9 %copy-start.1 = (bf16[512,512]{1,0:T(8,128)(2,1)S(1)}, bf16[512,512]{1,0:T(8,128)(2,1)}, u32[]{:S(2)}) copy-start(bf16[512,512]{1,0:T(8,128)(2,1)} %constant.2.clone.back_ref) | copy-start | bytes 1572868

commit v5 on v4

--- a/solution.py
+++ b/solution.py
@@ -43,8 +43,8 @@
     head, lane = iota((8, 128), 0), iota((8, 128), 1)
     put_beta = ((lane == head) | (lane == head + 16)).astype(f32).astype(bf16)
     put_decay = ((lane == head + 8) | (lane == head + 24)).astype(f32).astype(bf16)
-    copies[0].wait()
-    copies[1].wait()
+    for copy in copies:
+        copy.wait()
     gain = jnp.sum(jnp.where(eye, gain_ref[...], 0.0), axis=1, keepdims=True)
     raw = jnp.concatenate([tok_ref[t] for t in range(4)], axis=1).astype(f32)
     scaled = raw * gain
@@ -53,13 +53,9 @@
     sub = iota((16, 512), 0)
     extra = jnp.where(sub < 2, high, jnp.where(sub < 4, squares - high, 0.0))
     moved = dot(jnp.concatenate([scaled, extra], axis=0).astype(bf16), pick, 1, 0)
-    copies[5].wait()
-    copies[6].wait()
     small = dot(beta_ref[...], put_beta, 0, 0) + dot(decay_ref[...], put_decay, 0, 0)
     lane = iota((8, 128), 1)
     even = iota((8, 128), 0) % 2 == 0
-    for n in (2, 3, 4, 7):
-        copies[n].wait()
     for r in range(8):
         at = slice(128 * (r // 2), 128 * (r // 2) + 128)
         sums = moved[32:40, at]
@@ -224,8 +220,12 @@
 
 
 def place_kernel(x_ref, back_ref, states_ref, out_ref, kept_ref, sem):
-    copy = pltpu.make_async_copy(states_ref, kept_ref, sem)
-    copy.start()
+    copies = [
+        pltpu.make_async_copy(states_ref.at[n // 4, n % 4], kept_ref.at[n // 4, n % 4], sem.at[n])
+        for n in range(8)
+    ]
+    for copy in copies:
+        copy.start()
     low = iota((16, 128), 1) < 64
     sums = [x_ref[2 * r].astype(f32) + x_ref[2 * r + 1].astype(f32) for r in range(8)]
     tiles = []
@@ -237,7 +237,8 @@
     whole = dot(jnp.concatenate(tiles, axis=1), back_ref[...], 1, 0).astype(bf16)
     for t in range(4):
         out_ref[t] = whole[:, 128 * t : 128 * t + 128]
-    copy.wait()
+    for copy in copies:
+        copy.wait()
 
 
 def back_table():
@@ -340,7 +341,7 @@
         place_kernel,
         (shape((4, 32, 128), bf16), shape(states.shape, f32)),
         (back, jnp.asarray(back_table()), states),
-        scratch=[pltpu.SemaphoreType.DMA],
+        scratch=[pltpu.SemaphoreType.DMA((8,))],
         outs=(VMEM, HBM),
         name="place",
     )

time: 87.2 us -> 87.2 us (level)
  no operation moved by 1% of the time
where the time goes in v5:
time: 87.2 us; the launch traced here: 86.9 us
  blocking collectives  80.6 us (92%)
  Pallas kernels  5.55 us (6%)
    all_to_all x4, blocking collectives, swap(): return lax.all_to_all(x, axes, 0, 0, tiled=True)  80.6 us
    pallas_call x5, Pallas kernels, call(): pl.pallas_call(kernel, out_shape=shapes, in_specs=specs or [VMEM] * len(a...  5.55 us

profile of v5, /device:TPU:1, one launch (start us, length us, event | category | flops | bytes accessed | tf_op | source)
XLA Modules:
  0.0 86.9 jit_solution(13937171363180688062)
XLA Ops:
  0.6 1.3 %pack.1 = bf16[8,32,2176]{2,1,0:T(8,128)(2,1)S(1)} custom-call(bf16[4,32,128]{2,1,0:T(8,128)(2,1)} %bitcast.18, f32[1,32]{1,0:T(1,128)} %bitcast.22, bf16[32,512]{1,0:T(8,128)(2,1)} %refs_2_.1, bf16[32,512]{1,0:T(8,128)(2,1)} %refs_3_.1, bf16[32,512]{1,0:T(8,128)(2,1)} %refs_4_.1, bf16[8,32]{1,0:T(8,128)(2,1)} %bitcast.20, bf16[8,32]{1,0:T(8,128)(2,1)} %bitcast.21, ...), custom_call_target="tpu_custom_call" | custom-call | tf_op jit(solution)/shard_map/pack/pallas_call | solution.py:254
  2.0 19.4 %all_to_all.20.x_ref = bf16[8,32,2176]{2,1,0:T(8,128)(2,1)S(1)} all-to-all(bf16[8,32,2176]{2,1,0:T(8,128)(2,1)S(1)} %pack.1), channel_id=1, replica_groups=mesh['dp'=4,'z8'=8,'zp'=2,'y'=4,'tp'=2] {'zp','y'}, dimensions={0} | all-to-all | bytes 2228224 | tf_op jit(solution)/shard_map/all_to_all | solution.py:285
  21.4 0.0 copy-start
  21.4 0.0 copy-start.2
  21.4 0.0 copy-start.3
  21.4 0.0 copy-start.4
  21.4 0.0 copy-start.5
  21.4 0.3 project.1
  21.7 32.6 %all_to_all.21 = bf16[8,8,1664]{2,1,0:T(8,128)(2,1)S(1)} all-to-all(bf16[8,8,1664]{2,1,0:T(8,128)(2,1)S(1)} %bitcast.13), channel_id=1, replica_groups=mesh['dp'=4,'z8'=8,'zp'=2,'y'=4,'tp'=2] {'z8'}, dimensions={0} | all-to-all | bytes 425984 | tf_op jit(solution)/shard_map/all_to_all | solution.py:285
  54.3 0.0 copy-done
  54.3 0.0 copy-done.2
  54.3 0.0 copy-done.3
  54.3 0.0 copy-done.4
  54.3 0.0 copy-done.5
  54.3 0.0 copy-start.1
  54.4 2.0 %delta.1 = (f32[2,4,8,4096]{3,2,1,0:T(8,128)S(1)}, bf16[64,512]{1,0:T(8,128)(2,1)S(1)}) custom-call(s32[2]{0:T(128)S(1)} %copy-done.3, bf16[64,1664]{1,0:T(8,128)(2,1)S(1)} %bitcast.12, f32[2,4,8,4096]{3,2,1,0:T(8,128)S(1)} %copy-done, f32[1,8]{1,0:T(1,128)S(1)} %bitcast.16, f32[2,4,8]{2,1,0:T(4,128)S(1)} %copy-done.2, f32[1,64]{1,0:T(1,128)S(1)} %bitcast.17), custom_call_target="tpu_custom_call" | custom-call | tf_op jit(solution)/shard_map/delta/pallas_call | solution.py:254
  56.4 16.6 %all_to_all.22 = bf16[8,8,512]{2,1,0:T(8,128)(2,1)S(1)} all-to-all(bf16[8,8,512]{2,1,0:T(8,128)(2,1)S(1)} %bitcast.15), channel_id=1, replica_groups=mesh['dp'=4,'z8'=8,'zp'=2,'y'=4,'tp'=2] {'z8'}, dimensions={0} | all-to-all | bytes 131072 | tf_op jit(solution)/shard_map/all_to_all | solution.py:285
  73.0 0.2 mix.1
  73.2 12.0 %all_to_all.23.x_ref = bf16[16,16,128]{2,1,0:T(8,128)(2,1)S(1)} all-to-all(bf16[16,16,128]{2,1,0:T(8,128)(2,1)S(1)} %mix.1), channel_id=1, replica_groups=mesh['dp'=4,'z8'=8,'zp'=2,'y'=4,'tp'=2] {'zp','y','tp'}, dimensions={0} | all-to-all | bytes 131072 | tf_op jit(solution)/shard_map/all_to_all | solution.py:285
  85.2 0.0 copy-done.1
  85.2 1.7 %place.1 = (bf16[4,32,128]{2,1,0:T(8,128)(2,1)}, f32[2,4,8,4096]{3,2,1,0:T(8,128)}) custom-call(bf16[16,16,128]{2,1,0:T(8,128)(2,1)S(1)} %all_to_all.23.x_ref, bf16[512,512]{1,0:T(8,128)(2,1)S(1)} %copy-done.1, f32[2,4,8,4096]{3,2,1,0:T(8,128)S(1)} %get-tuple-element.7.states_ref), custom_call_target="tpu_custom_call" | custom-call | tf_op jit(solution)/shard_map/place/pallas_call | solution.py:254
Async XLA Ops:
  21.4 32.9 %copy-start = (f32[2,4,8,4096]{3,2,1,0:T(8,128)S(1)}, f32[2,4,8,4096]{3,2,1,0:T(8,128)}, u32[]{:S(2)}) copy-start(f32[2,4,8,4096]{3,2,1,0:T(8,128)} %prior_ref.1) | copy-start | bytes 3145732
  21.4 32.9 %copy-start.2 = (f32[2,4,8]{2,1,0:T(4,128)S(1)}, f32[2,4,8]{2,1,0:T(4,128)}, u32[]{:S(2)}) copy-start(f32[2,4,8]{2,1,0:T(4,128)} %extra_ref.1) | copy-start | bytes 772
  21.4 32.9 %copy-start.3 = (s32[2]{0:T(128)S(1)}, s32[2]{0:T(128)}, u32[]{:S(2)}) copy-start(s32[2]{0:T(128)} %accepted_ref.1) | copy-start | bytes 28
  21.4 32.9 %copy-start.4 = (f32[8]{0:T(128)S(1)}, f32[8]{0:T(128)}, u32[]{:S(2)}) copy-start(f32[8]{0:T(128)} %param.21) | copy-start | bytes 100
  21.4 33.0 %copy-start.5 = (f32[64]{0:T(128)S(1)}, f32[64]{0:T(128)}, u32[]{:S(2)}) copy-start(f32[64]{0:T(128)} %param.25) | copy-start | bytes 772
  54.3 30.9 %copy-start.1 = (bf16[512,512]{1,0:T(8,128)(2,1)S(1)}, bf16[512,512]{1,0:T(8,128)(2,1)}, u32[]{:S(2)}) copy-start(bf16[512,512]{1,0:T(8,128)(2,1)} %constant.2.clone.back_ref) | copy-start | bytes 1572868

commit v6 on v5

--- a/solution.py
+++ b/solution.py
@@ -99,8 +99,8 @@
 
 
 def delta_kernel(
-    accepted_ref, c_ref, prior_ref, rate_ref, extra_ref, gain_ref, states_ref, rows_ref,
-    aux, nrows, kept
+    accepted_ref, c_ref, prior_ref, rate_ref, extra_ref, gain_ref, out_ref, late_ref, rows_ref,
+    aux, nrows, kept, begin, early_ref, sems
 ):
     c = c_ref[...].astype(f32)
     s = (c[0:8] + c[8:16]) + (c[16:24] + c[24:32])
@@ -137,23 +137,31 @@
     def half_sum(values):
         return 0.5 * jnp.sum(values, axis=1, keepdims=True)
 
-    def unit(values):
-        return values * lax.rsqrt(half_sum(values * values) + epsilon)
+    def norm(values):
+        return lax.rsqrt(half_sum(values * values) + epsilon)
 
     ROWS = range(8)
-    q = [unit(by_heads(parts[0], row)) * 0.125 for row in ROWS]
-    k = [unit(by_heads(parts[1], row)) for row in ROWS]
+    q = [by_heads(parts[0], row) for row in ROWS]
+    k = [by_heads(parts[1], row) for row in ROWS]
     v = [by_heads(parts[2], row) for row in ROWS]
+    q_norm = [norm(values) * 0.125 for values in q]
+    k_norm = [norm(values) for values in k]
     a = [jnp.broadcast_to(fade[:, row : row + 1], (8, 128)) for row in ROWS]
     b = [jnp.broadcast_to(beta[:, row : row + 1], (8, 128)) for row in ROWS]
 
-    starts = [accepted_ref[0] - 1, accepted_ref[1] - 1]
+    is_step = []
+    for j in range(2):
+        taken = jnp.broadcast_to(accepted_ref[0:1, j : j + 1], (8, 128))
+        is_step.append([taken == n + 1 for n in range(3)])
     ks, qs = [None] * 8, [None] * 8
     for i in range(32):
         index = lane // 64 + 2 * i
         at = slice(128 * i, 128 * i + 128)
         for j in range(2):
-            start = prior_ref[j, starts[j], :, at]
+            start = prior_ref[j, 3, :, at]
+            for n in range(3):
+                start = jnp.where(is_step[j][n], prior_ref[j, n, :, at], start)
+            begin[j, :, at] = start
             for row in range(4 * j, 4 * j + 4):
                 kx = jnp.take_along_axis(k[row], index, axis=1, mode="promise_in_bounds")
                 qx = jnp.take_along_axis(q[row], index, axis=1, mode="promise_in_bounds")
@@ -164,48 +172,52 @@
     def fold(values):
         return values + pltpu.roll(values, 64, 1)
 
-    ks = [fold(values) for values in ks]
-    qs = [fold(values) for values in qs]
-    w, o = [None] * 8, [None] * 8
+    copies = []
     for j in range(2):
-        base = 4 * j
+        w, kw = [None] * 4, [None] * 4
         grown = None
         for t in range(4):
-            row = base + t
-            carried = ks[row] if t == 0 else grown * ks[row]
+            row = 4 * j + t
+            read = k_norm[row] * fold(ks[row])
+            carried = read if t == 0 else grown * read
             for e in range(t):
-                reach = half_sum(k[row] * k[base + e])
+                reach = half_sum(k[row] * k[4 * j + e]) * k_norm[row]
                 for m in range(e + 1, t):
-                    reach = reach * a[base + m]
-                carried = carried + reach * w[base + e]
-            w[row] = b[row] * (v[row] - a[row] * carried)
+                    reach = reach * a[4 * j + m]
+                carried = carried + reach * kw[e]
+            w[t] = b[row] * (v[row] - a[row] * carried)
+            kw[t] = k_norm[row] * w[t]
             grown = a[row] if t == 0 else grown * a[row]
-            out = grown * qs[row] + half_sum(q[row] * k[row]) * w[row]
-            for e in range(t):
-                reach = half_sum(q[row] * k[base + e])
+            out = grown * (q_norm[row] * fold(qs[row]))
+            for e in range(t + 1):
+                reach = half_sum(q[row] * k[4 * j + e]) * q_norm[row]
                 for m in range(e + 1, t + 1):
-                    reach = reach * a[base + m]
-                out = out + reach * w[base + e]
-            o[row] = out
-
-    for j in range(2):
+                    reach = reach * a[4 * j + m]
+                out = out + reach * kw[e]
+            mean = half_sum(out * out) / 64
+            n = out * lax.rsqrt(mean + epsilon) * gain
+            for p in range(4):
+                nrows[row : row + 1, 128 * p : 128 * p + 128] = jnp.sum(
+                    jnp.where(masks[p], n, 0.0), axis=0, keepdims=True
+                )
+        states_ref = early_ref if j == 0 else late_ref
         for i in range(32):
             at = slice(128 * i, 128 * i + 128)
-            state = prior_ref[j, starts[j], :, at]
+            state = begin[j, :, at]
             for t in range(4):
                 row = 4 * j + t
-                state = a[row] * state + kept[row, :, at] * w[row]
-                states_ref[j, t, :, at] = state
-
-    for row in ROWS:
-        mean = half_sum(o[row] * o[row]) / 64
-        n = o[row] * lax.rsqrt(mean + epsilon) * gain
-        for p in range(4):
-            nrows[row : row + 1, 128 * p : 128 * p + 128] = jnp.sum(
-                jnp.where(masks[p], n, 0.0), axis=0, keepdims=True
-            )
+                state = a[row] * state + kept[row, :, at] * kw[t]
+                states_ref[t, :, at] = state
+        if j == 0:
+            for t in range(4):
+                copies.append(
+                    pltpu.make_async_copy(early_ref.at[t], out_ref.at[0, t], sems.at[t])
+                )
+                copies[-1].start()
     rows = nrows[...]
     rows_ref[...] = jnp.concatenate([rows] * 8, axis=0).astype(bf16)
+    for copy in copies:
+        copy.wait()
 
 
 def mix_kernel(x_ref, rows_ref, out_ref):
@@ -219,10 +231,9 @@
         out_ref[2 * r + 1] = piece.astype(bf16)
 
 
-def place_kernel(x_ref, back_ref, states_ref, out_ref, kept_ref, sem):
+def place_kernel(x_ref, back_ref, late_ref, begun_ref, out_ref, whole_ref, sems):
     copies = [
-        pltpu.make_async_copy(states_ref.at[n // 4, n % 4], kept_ref.at[n // 4, n % 4], sem.at[n])
-        for n in range(8)
+        pltpu.make_async_copy(late_ref.at[t], whole_ref.at[1, t], sems.at[t]) for t in range(4)
     ]
     for copy in copies:
         copy.start()
@@ -248,7 +259,7 @@
     return (wanted[:, None] == np.arange(512)[None, :]).astype(jnp.bfloat16)
 
 
-def call(kernel, shapes, args, specs=None, scratch=(), outs=VMEM, name=None):
+def call(kernel, shapes, args, specs=None, scratch=(), outs=VMEM, name=None, aliases=None):
     if name == "pack":
         args = [pltpu.with_memory_space_constraint(a, pltpu.HBM) for a in args]
     return pl.pallas_call(
@@ -258,6 +269,7 @@
         out_specs=outs,
         scratch_shapes=scratch,
         compiler_params=pltpu.CompilerParams(vmem_limit_bytes=16 << 20),
+        input_output_aliases=aliases or {},
         name=name,
     )(*args)
 
@@ -314,38 +326,46 @@
     near = swap(packed, NEAR)
     part = call(project_kernel, shape((64, WIDE - QKV), bf16), (near,), name="project")
     arrived = swap(part.reshape(8, 8, part.shape[1]), "z8").reshape(part.shape)
-    states, rows = call(
+    begun, late, rows = call(
         delta_kernel,
-        (shape(prior_step_states.shape, f32), shape((64, 512), bf16)),
         (
-            accepted,
+            shape(prior_step_states.shape, f32),
+            shape(prior_step_states.shape[1:], f32),
+            shape((64, 512), bf16),
+        ),
+        (
+            accepted[None, :],
             arrived,
             prior_step_states,
             head_decay_rate[None, :],
             token_extra_decay,
             output_norm_gain[None, :],
         ),
-        specs=[SMEM] + [VMEM] * 5,
         scratch=[
             pltpu.VMEM((8, 128), f32),
             pltpu.VMEM((8, 512), f32),
             pltpu.VMEM((8, 8, 4096), f32),
+            pltpu.VMEM((2, 8, 4096), f32),
+            pltpu.VMEM((4, 8, 4096), f32),
+            pltpu.SemaphoreType.DMA((4,)),
         ],
-        outs=(VMEM, VMEM),
+        outs=(HBM, VMEM, VMEM),
         name="delta",
     )
     all_rows = swap(rows.reshape(8, 8, 512), "z8").reshape(64, 512)
     columns = call(mix_kernel, shape((16, 16, 128), bf16), (near, all_rows), name="mix")
     back = swap(columns, ("zp", "y", "tp"))
-    mixed, kept = call(
+    mixed, whole = call(
         place_kernel,
-        (shape((4, 32, 128), bf16), shape(states.shape, f32)),
-        (back, jnp.asarray(back_table()), states),
-        scratch=[pltpu.SemaphoreType.DMA((8,))],
+        (shape((4, 32, 128), bf16), shape(begun.shape, f32)),
+        (back, jnp.asarray(back_table()), late, begun),
+        specs=[VMEM, VMEM, VMEM, HBM],
+        scratch=[pltpu.SemaphoreType.DMA((4,))],
         outs=(VMEM, HBM),
+        aliases={3: 1},
         name="place",
     )
-    return (jnp.transpose(mixed, (2, 0, 1)), kept)
+    return (jnp.transpose(mixed, (2, 0, 1)), whole)
 
 
 def solution(mesh):

time: 87.2 us -> 87.4 us (level)
  no operation moved by 1% of the time
where the time goes in v6:
time: 87.4 us; the launch traced here: 87 us
  blocking collectives  80.6 us (92%)
  Pallas kernels  5.66 us (6%)
    all_to_all x4, blocking collectives, swap(): return lax.all_to_all(x, axes, 0, 0, tiled=True)  80.6 us
    pallas_call x5, Pallas kernels, call(): pl.pallas_call(kernel, out_shape=shapes, in_specs=specs or [VMEM] * len(a...  5.66 us

profile of v6, /device:TPU:1, one launch (start us, length us, event | category | flops | bytes accessed | tf_op | source)
XLA Modules:
  0.0 87.0 jit_solution(10018966955781859644)
XLA Ops:
  0.6 1.3 %pack.1 = bf16[8,32,2176]{2,1,0:T(8,128)(2,1)S(1)} custom-call(bf16[4,32,128]{2,1,0:T(8,128)(2,1)} %bitcast.20, f32[1,32]{1,0:T(1,128)} %bitcast.24, bf16[32,512]{1,0:T(8,128)(2,1)} %refs_2_.1, bf16[32,512]{1,0:T(8,128)(2,1)} %refs_3_.1, bf16[32,512]{1,0:T(8,128)(2,1)} %refs_4_.1, bf16[8,32]{1,0:T(8,128)(2,1)} %bitcast.22, bf16[8,32]{1,0:T(8,128)(2,1)} %bitcast.23, ...), custom_call_target="tpu_custom_call" | custom-call | tf_op jit(solution)/shard_map/pack/pallas_call | solution.py:265
  2.0 19.4 %all_to_all.20.x_ref = bf16[8,32,2176]{2,1,0:T(8,128)(2,1)S(1)} all-to-all(bf16[8,32,2176]{2,1,0:T(8,128)(2,1)S(1)} %pack.1), channel_id=1, replica_groups=mesh['dp'=4,'z8'=8,'zp'=2,'y'=4,'tp'=2] {'zp','y'}, dimensions={0} | all-to-all | bytes 2228224 | tf_op jit(solution)/shard_map/all_to_all | solution.py:297
  21.4 0.0 copy-start
  21.4 0.0 copy-start.2
  21.4 0.0 copy-start.3
  21.4 0.0 copy-start.4
  21.4 0.0 copy-start.5
  21.4 0.3 project.1
  21.7 32.6 %all_to_all.21 = bf16[8,8,1664]{2,1,0:T(8,128)(2,1)S(1)} all-to-all(bf16[8,8,1664]{2,1,0:T(8,128)(2,1)S(1)} %bitcast.14), channel_id=1, replica_groups=mesh['dp'=4,'z8'=8,'zp'=2,'y'=4,'tp'=2] {'z8'}, dimensions={0} | all-to-all | bytes 425984 | tf_op jit(solution)/shard_map/all_to_all | solution.py:297
  54.3 0.0 copy-done
  54.3 0.0 copy-done.2
  54.3 0.0 copy-done.3
  54.3 0.0 copy-done.4
  54.3 0.0 copy-done.5
  54.3 0.0 copy-start.1
  54.4 2.3 %delta.1 = (f32[2,4,8,4096]{3,2,1,0:T(8,128)}, f32[4,8,4096]{2,1,0:T(8,128)S(1)}, bf16[64,512]{1,0:T(8,128)(2,1)S(1)}) custom-call(s32[1,2]{1,0:T(1,128)S(1)} %bitcast.17, bf16[64,1664]{1,0:T(8,128)(2,1)S(1)} %bitcast.13, f32[2,4,8,4096]{3,2,1,0:T(8,128)S(1)} %copy-done, f32[1,8]{1,0:T(1,128)S(1)} %bitcast.18, f32[2,4,8]{2,1,0:T(4,128)S(1)} %copy-done.2, ...), custom_call_target="tpu_custom_call" | custom-call | tf_op jit(solution)/shard_map/delta/pallas_call | solution.py:265
  56.7 16.6 %all_to_all.22 = bf16[8,8,512]{2,1,0:T(8,128)(2,1)S(1)} all-to-all(bf16[8,8,512]{2,1,0:T(8,128)(2,1)S(1)} %bitcast.16), channel_id=1, replica_groups=mesh['dp'=4,'z8'=8,'zp'=2,'y'=4,'tp'=2] {'z8'}, dimensions={0} | all-to-all | bytes 131072 | tf_op jit(solution)/shard_map/all_to_all | solution.py:297
  73.3 0.2 mix.1
  73.6 12.0 %all_to_all.23.x_ref = bf16[16,16,128]{2,1,0:T(8,128)(2,1)S(1)} all-to-all(bf16[16,16,128]{2,1,0:T(8,128)(2,1)S(1)} %mix.1), channel_id=1, replica_groups=mesh['dp'=4,'z8'=8,'zp'=2,'y'=4,'tp'=2] {'zp','y','tp'}, dimensions={0} | all-to-all | bytes 131072 | tf_op jit(solution)/shard_map/all_to_all | solution.py:297
  85.6 0.0 copy-done.1
  85.6 1.5 %place.1 = (bf16[4,32,128]{2,1,0:T(8,128)(2,1)}, f32[2,4,8,4096]{3,2,1,0:T(8,128)}) custom-call(bf16[16,16,128]{2,1,0:T(8,128)(2,1)S(1)} %all_to_all.23.x_ref, bf16[512,512]{1,0:T(8,128)(2,1)S(1)} %copy-done.1, f32[4,8,4096]{2,1,0:T(8,128)S(1)} %get-tuple-element.8.late_ref, ...), custom_call_target="tpu_custom_call", output_to_operand_aliasing={{1}: (3, {})} | custom-call | tf_op jit(solution)/shard_map/place/pallas_call | solution.py:265
Async XLA Ops:
  21.4 32.9 %copy-start = (f32[2,4,8,4096]{3,2,1,0:T(8,128)S(1)}, f32[2,4,8,4096]{3,2,1,0:T(8,128)}, u32[]{:S(2)}) copy-start(f32[2,4,8,4096]{3,2,1,0:T(8,128)} %prior_ref.1) | copy-start | bytes 3145732
  21.4 32.9 %copy-start.2 = (f32[2,4,8]{2,1,0:T(4,128)S(1)}, f32[2,4,8]{2,1,0:T(4,128)}, u32[]{:S(2)}) copy-start(f32[2,4,8]{2,1,0:T(4,128)} %extra_ref.1) | copy-start | bytes 772
  21.4 32.9 %copy-start.3 = (s32[2]{0:T(128)S(1)}, s32[2]{0:T(128)}, u32[]{:S(2)}) copy-start(s32[2]{0:T(128)} %param.23) | copy-start | bytes 28
  21.4 32.9 %copy-start.4 = (f32[8]{0:T(128)S(1)}, f32[8]{0:T(128)}, u32[]{:S(2)}) copy-start(f32[8]{0:T(128)} %param.21) | copy-start | bytes 100
  21.4 33.0 %copy-start.5 = (f32[64]{0:T(128)S(1)}, f32[64]{0:T(128)}, u32[]{:S(2)}) copy-start(f32[64]{0:T(128)} %param.25) | copy-start | bytes 772
  54.3 31.2 %copy-start.1 = (bf16[512,512]{1,0:T(8,128)(2,1)S(1)}, bf16[512,512]{1,0:T(8,128)(2,1)}, u32[]{:S(2)}) copy-start(bf16[512,512]{1,0:T(8,128)(2,1)} %constant.2.clone.back_ref) | copy-start | bytes 1572868

commit v7 on v5

--- a/solution.py
+++ b/solution.py
@@ -219,13 +219,7 @@
         out_ref[2 * r + 1] = piece.astype(bf16)
 
 
-def place_kernel(x_ref, back_ref, states_ref, out_ref, kept_ref, sem):
-    copies = [
-        pltpu.make_async_copy(states_ref.at[n // 4, n % 4], kept_ref.at[n // 4, n % 4], sem.at[n])
-        for n in range(8)
-    ]
-    for copy in copies:
-        copy.start()
+def place_kernel(x_ref, back_ref, out_ref):
     low = iota((16, 128), 1) < 64
     sums = [x_ref[2 * r].astype(f32) + x_ref[2 * r + 1].astype(f32) for r in range(8)]
     tiles = []
@@ -237,8 +231,6 @@
     whole = dot(jnp.concatenate(tiles, axis=1), back_ref[...], 1, 0).astype(bf16)
     for t in range(4):
         out_ref[t] = whole[:, 128 * t : 128 * t + 128]
-    for copy in copies:
-        copy.wait()
 
 
 def back_table():
@@ -248,7 +240,7 @@
     return (wanted[:, None] == np.arange(512)[None, :]).astype(jnp.bfloat16)
 
 
-def call(kernel, shapes, args, specs=None, scratch=(), outs=VMEM, name=None):
+def call(kernel, shapes, args, specs=None, scratch=(), outs=VMEM, name=None, aliases=None):
     if name == "pack":
         args = [pltpu.with_memory_space_constraint(a, pltpu.HBM) for a in args]
     return pl.pallas_call(
@@ -258,6 +250,7 @@
         out_specs=outs,
         scratch_shapes=scratch,
         compiler_params=pltpu.CompilerParams(vmem_limit_bytes=16 << 20),
+        input_output_aliases=aliases or {},
         name=name,
     )(*args)
 
@@ -316,7 +309,7 @@
     arrived = swap(part.reshape(8, 8, part.shape[1]), "z8").reshape(part.shape)
     states, rows = call(
         delta_kernel,
-        (shape(prior_step_states.shape, f32), shape((64, 512), bf16)),
+        (pltpu.VMEM(prior_step_states.shape, f32), shape((64, 512), bf16)),
         (
             accepted,
             arrived,
@@ -337,15 +330,10 @@
     all_rows = swap(rows.reshape(8, 8, 512), "z8").reshape(64, 512)
     columns = call(mix_kernel, shape((16, 16, 128), bf16), (near, all_rows), name="mix")
     back = swap(columns, ("zp", "y", "tp"))
-    mixed, kept = call(
-        place_kernel,
-        (shape((4, 32, 128), bf16), shape(states.shape, f32)),
-        (back, jnp.asarray(back_table()), states),
-        scratch=[pltpu.SemaphoreType.DMA((8,))],
-        outs=(VMEM, HBM),
-        name="place",
-    )
-    return (jnp.transpose(mixed, (2, 0, 1)), kept)
+    mixed = call(
+        place_kernel, shape((4, 32, 128), bf16), (back, jnp.asarray(back_table())), name="place"
+    )
+    return (jnp.transpose(mixed, (2, 0, 1)), states)
 
 
 def solution(mesh):

time: 87.2 us -> 87.4 us (level)
  blocking collectives: 80.6 us -> 68.6 us
  starting transfers between devices: 0 us -> 6.52 us
  waiting for transfers between devices: 0 us -> 4.85 us
  local copies, waits for them, and re-layouts: 0.03 us -> 0.99 us
    all_to_all x4 -> x3, blocking collectives: 80.6 us -> 68.6 us  [swap(): return lax.all_to_all(x, axes, 0, 0, tiled=True)]
    all_to_all x0 -> x1, starting transfers between devices: none -> 6.52 us  [swap(): return lax.all_to_all(x, axes, 0, 0, tiled=True)]
    all_to_all x0 -> x1, waiting for transfers between devices: none -> 4.85 us  [swap(): return lax.all_to_all(x, axes, 0, 0, tiled=True)]
    unnamed x12 -> x13, local copies, waits for them, and re-layouts: 0.03 us -> 0.99 us
  transfers between devices with their start and end apart: 0 -> 1, of which waited for: 0 -> 1; matrix products, arithmetic and copies ran while one was open for 0% -> 1% of each run, Pallas kernels for 0% -> 0%
where the time goes in v7:
time: 87.4 us; the launch traced here: 87.1 us
  blocking collectives  68.6 us (78%)
  starting transfers between devices  6.52 us (7%)
  Pallas kernels  5.37 us (6%)
  waiting for transfers between devices  4.85 us (6%)
  local copies, waits for them, and re-layouts  0.99 us (1%)
    all_to_all x3, blocking collectives, swap(): return lax.all_to_all(x, axes, 0, 0, tiled=True)  68.6 us
    all_to_all x1, starting transfers between devices, swap(): return lax.all_to_all(x, axes, 0, 0, tiled=True)  6.52 us
    pallas_call x5, Pallas kernels, call(): pl.pallas_call(kernel, out_shape=shapes, in_specs=specs or [VMEM] * len(a...  5.37 us
    all_to_all x1, waiting for transfers between devices, swap(): return lax.all_to_all(x, axes, 0, 0, tiled=True)  4.85 us
  transfers between devices with their start and end apart: 1, of which 1 were waited for; matrix products, arithmetic and copies ran while one was open for 1% of the time, Pallas kernels for 0%

profile of v7, /device:TPU:1, one launch (start us, length us, event | category | flops | bytes accessed | tf_op | source)
XLA Modules:
  0.0 87.1 jit_solution(2073598769615232096)
XLA Ops:
  0.6 1.3 %pack.1 = bf16[8,32,2176]{2,1,0:T(8,128)(2,1)S(1)} custom-call(bf16[4,32,128]{2,1,0:T(8,128)(2,1)} %bitcast.18, f32[1,32]{1,0:T(1,128)} %bitcast.23, bf16[32,512]{1,0:T(8,128)(2,1)} %refs_2_.1, bf16[32,512]{1,0:T(8,128)(2,1)} %refs_3_.1, bf16[32,512]{1,0:T(8,128)(2,1)} %refs_4_.1, bf16[8,32]{1,0:T(8,128)(2,1)} %bitcast.21, bf16[8,32]{1,0:T(8,128)(2,1)} %bitcast.22, ...), custom_call_target="tpu_custom_call" | custom-call | tf_op jit(solution)/shard_map/pack/pallas_call | solution.py:246
  2.0 19.4 %all_to_all.20.x_ref = bf16[8,32,2176]{2,1,0:T(8,128)(2,1)S(1)} all-to-all(bf16[8,32,2176]{2,1,0:T(8,128)(2,1)S(1)} %pack.1), channel_id=1, replica_groups=mesh['dp'=4,'z8'=8,'zp'=2,'y'=4,'tp'=2] {'zp','y'}, dimensions={0} | all-to-all | bytes 2228224 | tf_op jit(solution)/shard_map/all_to_all | solution.py:278
  21.4 0.0 copy-start
  21.4 0.0 copy-start.2
  21.4 0.0 copy-start.3
  21.4 0.0 copy-start.4
  21.4 0.0 copy-start.5
  21.4 0.3 project.1
  21.7 32.6 %all_to_all.21 = bf16[8,8,1664]{2,1,0:T(8,128)(2,1)S(1)} all-to-all(bf16[8,8,1664]{2,1,0:T(8,128)(2,1)S(1)} %bitcast.13), channel_id=1, replica_groups=mesh['dp'=4,'z8'=8,'zp'=2,'y'=4,'tp'=2] {'z8'}, dimensions={0} | all-to-all | bytes 425984 | tf_op jit(solution)/shard_map/all_to_all | solution.py:278
  54.3 0.0 copy-done
  54.3 0.0 copy-done.2
  54.3 0.0 copy-done.3
  54.3 0.0 copy-done.4
  54.3 0.0 copy-done.5
  54.3 2.0 %delta.1 = (f32[2,4,8,4096]{3,2,1,0:T(8,128)S(1)}, bf16[64,512]{1,0:T(8,128)(2,1)S(1)}) custom-call(s32[2]{0:T(128)S(1)} %copy-done.3, bf16[64,1664]{1,0:T(8,128)(2,1)S(1)} %bitcast.12, f32[2,4,8,4096]{3,2,1,0:T(8,128)S(1)} %copy-done, f32[1,8]{1,0:T(1,128)S(1)} %bitcast.16, f32[2,4,8]{2,1,0:T(4,128)S(1)} %copy-done.2, f32[1,64]{1,0:T(1,128)S(1)} %bitcast.17), custom_call_target="tpu_custom_call" | custom-call | tf_op jit(solution)/shard_map/delta/pallas_call | solution.py:246
  56.4 16.6 %all_to_all.22 = bf16[8,8,512]{2,1,0:T(8,128)(2,1)S(1)} all-to-all(bf16[8,8,512]{2,1,0:T(8,128)(2,1)S(1)} %bitcast.15), channel_id=1, replica_groups=mesh['dp'=4,'z8'=8,'zp'=2,'y'=4,'tp'=2] {'z8'}, dimensions={0} | all-to-all | bytes 131072 | tf_op jit(solution)/shard_map/all_to_all | solution.py:278
  73.0 0.9 mix.1
  73.9 0.0 copy-start.1
  73.9 6.5 %all-to-all-start.3 = ((bf16[16,16,128]{2,1,0:T(8,128)(2,1)}), bf16[16,16,128]{2,1,0:T(8,128)(2,1)S(1)}, u32[]{:S(2)}, u32[]{:S(2)}) async-start(bf16[16,16,128]{2,1,0:T(8,128)(2,1)} %mix.1), calls=%async_computation.3 | async-start | bytes 131072 | tf_op jit(solution)/shard_map/all_to_all | solution.py:278
  80.4 1.0 %copy.16 = f32[2,4,8,4096]{3,2,1,0:T(8,128)} copy(f32[2,4,8,4096]{3,2,1,0:T(8,128)S(1)} %get-tuple-element.7) | data formatting | bytes 2097152
  81.4 4.9 %all-to-all-done.3.x_ref = bf16[16,16,128]{2,1,0:T(8,128)(2,1)S(1)} async-done(((bf16[16,16,128]{2,1,0:T(8,128)(2,1)}), bf16[16,16,128]{2,1,0:T(8,128)(2,1)S(1)}, u32[]{:S(2)}, u32[]{:S(2)}) %all-to-all-start.3) | async-done | bytes 65568 | tf_op jit(solution)/shard_map/all_to_all | solution.py:278
  86.2 0.0 copy-done.1
  86.2 0.9 place.1
Async XLA Ops:
  21.4 32.9 %copy-start = (f32[2,4,8,4096]{3,2,1,0:T(8,128)S(1)}, f32[2,4,8,4096]{3,2,1,0:T(8,128)}, u32[]{:S(2)}) copy-start(f32[2,4,8,4096]{3,2,1,0:T(8,128)} %prior_ref.1) | copy-start | bytes 3145732
  21.4 32.9 %copy-start.2 = (f32[2,4,8]{2,1,0:T(4,128)S(1)}, f32[2,4,8]{2,1,0:T(4,128)}, u32[]{:S(2)}) copy-start(f32[2,4,8]{2,1,0:T(4,128)} %extra_ref.1) | copy-start | bytes 772
  21.4 32.9 %copy-start.3 = (s32[2]{0:T(128)S(1)}, s32[2]{0:T(128)}, u32[]{:S(2)}) copy-start(s32[2]{0:T(128)} %accepted_ref.1) | copy-start | bytes 28
  21.4 32.9 %copy-start.4 = (f32[8]{0:T(128)S(1)}, f32[8]{0:T(128)}, u32[]{:S(2)}) copy-start(f32[8]{0:T(128)} %param.21) | copy-start | bytes 100
  21.4 33.0 %copy-start.5 = (f32[64]{0:T(128)S(1)}, f32[64]{0:T(128)}, u32[]{:S(2)}) copy-start(f32[64]{0:T(128)} %param.25) | copy-start | bytes 772
  73.9 12.3 %copy-start.1 = (bf16[512,512]{1,0:T(8,128)(2,1)S(1)}, bf16[512,512]{1,0:T(8,128)(2,1)}, u32[]{:S(2)}) copy-start(bf16[512,512]{1,0:T(8,128)(2,1)} %constant.2.clone.back_ref) | copy-start | bytes 1572868
  73.9 12.3 %all-to-all-start.3 = ((bf16[16,16,128]{2,1,0:T(8,128)(2,1)}), bf16[16,16,128]{2,1,0:T(8,128)(2,1)S(1)}, u32[]{:S(2)}, u32[]{:S(2)}) async-start(bf16[16,16,128]{2,1,0:T(8,128)(2,1)} %mix.1), calls=%async_computation.3 | async-start | bytes 131072 | tf_op jit(solution)/shard_map/all_to_all | solution.py:278

commit v8 on v5

--- a/solution.py
+++ b/solution.py
@@ -1,3 +1,5 @@
+import functools
+
 import jax
 import jax.numpy as jnp
 import numpy as np
@@ -15,7 +17,7 @@
 f32 = jnp.float32
 bf16 = jnp.bfloat16
 
-WO, QKV, SMALL, WIDE = 0, 512, 2048, 2176
+QKV, SMALL, WO, WIDE = 0, 1536, 1664, 2176
 VMEM = pl.BlockSpec(memory_space=pltpu.VMEM)
 SMEM = pl.BlockSpec(memory_space=pltpu.SMEM)
 HBM = pl.BlockSpec(memory_space=pltpu.HBM)
@@ -29,8 +31,8 @@
     return lax.dot_general(a, b, (((ca,), (cb,)), ((), ())), preferred_element_type=f32)
 
 
-def pack_kernel(*refs):
-    hbm, out_ref, held, sems = refs[:8], refs[8], refs[9:17], refs[17]
+def pack_kernel(*refs, late):
+    hbm, out_ref, held, sems = refs[:8], refs[8], refs[-9:-1], refs[-1]
     copies = [pltpu.make_async_copy(hbm[n], held[n], sems.at[n]) for n in range(8)]
     for copy in copies:
         copy.start()
@@ -70,15 +72,20 @@
             right = jnp.where(lane < 64, sums if g == 0 else 0.0, cols[8 * g : 8 * g + 8])
             groups.append(jnp.where(lane < 32, small[8 * g : 8 * g + 8], right))
         tile = jnp.concatenate(groups, axis=0)
-        out_ref[r, :, WO:QKV] = wo_ref[...]
+        if late:
+            refs[9][r] = wo_ref[...]
+        else:
+            out_ref[r, :, WO:] = wo_ref[...]
         out_ref[r, :, QKV : QKV + 512] = q_ref[...]
         out_ref[r, :, QKV + 512 : QKV + 1024] = k_ref[...]
         out_ref[r, :, QKV + 1024 : SMALL] = v_ref[...]
-        out_ref[r, :, SMALL:] = tile.astype(bf16)
-
-
-def project_kernel(x_ref, out_ref):
-    x = x_ref[...].reshape(256, WIDE)
+        out_ref[r, :, SMALL:WO] = tile.astype(bf16)
+
+
+def project_kernel(x_ref, out_ref, *wo_refs):
+    for wo_ref in wo_refs:
+        wo_ref[...] = x_ref[:, :, WO:]
+    x = x_ref[:, :, :WO].reshape(256, WO)
     cols = x[:, SMALL:]
     main = dot(cols, x[:, QKV:SMALL], 0, 0)
     out_ref[:, : SMALL - QKV] = main[64:].astype(bf16)
@@ -209,7 +216,7 @@
 
 
 def mix_kernel(x_ref, rows_ref, out_ref):
-    w = x_ref[:, :, WO:QKV].reshape(256, 512)
+    w = x_ref[...].reshape(256, 512)
     rows = rows_ref[...]
     out = dot(w, jnp.concatenate([rows, rows], axis=0), 1, 1)
     low = iota((16, 128), 1) < 64
@@ -284,35 +291,58 @@
     def swap(x, axes):
         return lax.all_to_all(x, axes, 0, 0, tiled=True)
 
-    packed = call(
-        pack_kernel,
-        shape((8, 32, WIDE), bf16),
-        (
-            jnp.transpose(tokens, (1, 2, 0)),
-            input_norm_gain[None, :],
-            query_projection,
-            key_projection,
-            value_projection,
-            write_strength_weight.T,
-            decay_projection.T,
-            output_projection.T,
-        ),
-        specs=[HBM] * 8,
-        scratch=[
-            pltpu.VMEM((4, 32, 128), bf16),
-            pltpu.VMEM((1, 32), f32),
-            pltpu.VMEM((32, 512), bf16),
-            pltpu.VMEM((32, 512), bf16),
-            pltpu.VMEM((32, 512), bf16),
-            pltpu.VMEM((8, 32), bf16),
-            pltpu.VMEM((8, 32), bf16),
-            pltpu.VMEM((32, 512), bf16),
-            pltpu.SemaphoreType.DMA((8,)),
-        ],
-        name="pack",
-    )
-    near = swap(packed, NEAR)
-    part = call(project_kernel, shape((64, WIDE - QKV), bf16), (near,), name="project")
+    part_shape, wo_shape = shape((64, WO), bf16), shape((8, 32, 512), bf16)
+
+    def pack(late, args):
+        sizes = (shape((8, 32, WO), bf16), wo_shape) if late else shape((8, 32, WIDE), bf16)
+        return call(
+            functools.partial(pack_kernel, late=late),
+            sizes,
+            args,
+            specs=[HBM] * 8,
+            scratch=[
+                pltpu.VMEM((4, 32, 128), bf16),
+                pltpu.VMEM((1, 32), f32),
+                pltpu.VMEM((32, 512), bf16),
+                pltpu.VMEM((32, 512), bf16),
+                pltpu.VMEM((32, 512), bf16),
+                pltpu.VMEM((8, 32), bf16),
+                pltpu.VMEM((8, 32), bf16),
+                pltpu.VMEM((32, 512), bf16),
+                pltpu.SemaphoreType.DMA((8,)),
+            ],
+            outs=(VMEM, VMEM) if late else VMEM,
+            name="pack",
+        )
+
+    def start_late(*args):
+        packed, own = pack(True, args)
+        return call(project_kernel, part_shape, (swap(packed, NEAR),), name="project"), own
+
+    def start_early(*args):
+        near = swap(pack(False, args), NEAR)
+        return call(
+            project_kernel, (part_shape, wo_shape), (near,), outs=(VMEM, VMEM), name="project"
+        )
+
+    def mix(weights, rows):
+        return call(mix_kernel, shape((16, 16, 128), bf16), (weights, rows), name="mix")
+
+    pair = lax.axis_index("z8")
+    late = (pair >= 4) & (pair <= 6)
+    part, weights = lax.cond(
+        late,
+        start_late,
+        start_early,
+        jnp.transpose(tokens, (1, 2, 0)),
+        input_norm_gain[None, :],
+        query_projection,
+        key_projection,
+        value_projection,
+        write_strength_weight.T,
+        decay_projection.T,
+        output_projection.T,
+    )
     arrived = swap(part.reshape(8, 8, part.shape[1]), "z8").reshape(part.shape)
     states, rows = call(
         delta_kernel,
@@ -335,7 +365,9 @@
         name="delta",
     )
     all_rows = swap(rows.reshape(8, 8, 512), "z8").reshape(64, 512)
-    columns = call(mix_kernel, shape((16, 16, 128), bf16), (near, all_rows), name="mix")
+    columns = lax.cond(
+        late, lambda w, r: mix(swap(w, NEAR), r), lambda w, r: mix(w, r), weights, all_rows
+    )
     back = swap(columns, ("zp", "y", "tp"))
     mixed, kept = call(
         place_kernel,

time: 87.2 us -> 84.5 us (0.969)
  blocking collectives: 80.6 us -> 77.8 us
    all_to_all x4, blocking collectives: 80.6 us -> 77.8 us  [swap(): return lax.all_to_all(x, axes, 0, 0, tiled=True)]
where the time goes in v8:
time: 84.5 us; the launch traced here: 84.2 us
  blocking collectives  77.8 us (92%)
  Pallas kernels  5.6 us (7%)
    all_to_all x4, blocking collectives, swap(): return lax.all_to_all(x, axes, 0, 0, tiled=True)  77.8 us
    pallas_call x5, Pallas kernels, call(): pl.pallas_call(kernel, out_shape=shapes, in_specs=specs or [VMEM] * len(a...  5.6 us

profile of v8, /device:TPU:1, one launch (start us, length us, event | category | flops | bytes accessed | tf_op | source)
XLA Modules:
  0.0 84.2 jit_solution(13951336258273763030)
XLA Ops:
  0.6 0.0 copy-start
  0.7 0.0 copy-start.2
  0.7 0.0 copy-start.3
  0.7 0.0 copy-start.4
  0.7 0.0 copy-start.5
  0.7 21.1 %conditional.2 = ((bf16[64,1664]{1,0:T(8,128)(2,1)S(1)}, bf16[8,32,512]{2,1,0:T(8,128)(2,1)S(1)})) conditional(s32[]{:T(128)} %convert_element_type.4, (bf16[4,32,128]{2,1,0:T(8,128)(2,1)}, f32[1,32]{1,0:T(1,128)}, bf16[32,512]{1,0:T(8,128)(2,1)}, bf16[32,512]{1,0:T(8,128)(2,1)}, bf16[32,512]{1,0:T(8,128)(2,1)}, /*index=5*/bf16[8,32]{1,0:T(8,128)(2,1)}, ...), branch_computations={%region_0.0_spmd, %region_1.0_spmd} | conditional | bytes 2228232 | solution.py:333
  0.7 1.4 %pack.2 = bf16[8,32,2176]{2,1,0:T(8,128)(2,1)S(1)} custom-call(bf16[4,32,128]{2,1,0:T(8,128)(2,1)} %get-tuple-element.40.refs_0_, f32[1,32]{1,0:T(1,128)} %get-tuple-element.44.refs_1_, bf16[32,512]{1,0:T(8,128)(2,1)} %get-tuple-element.45.refs_2_, bf16[32,512]{1,0:T(8,128)(2,1)} %get-tuple-element.46.refs_3_, bf16[32,512]{1,0:T(8,128)(2,1)} %get-tuple-element.47.refs_4_, ...), custom_call_target="tpu_custom_call" | custom-call | tf_op jit(solution)/shard_map/cond/branch_0_fun/pack/pallas_call | solution.py:261
  2.1 19.4 %all_to_all.27.x_ref = bf16[8,32,2176]{2,1,0:T(8,128)(2,1)S(1)} all-to-all(bf16[8,32,2176]{2,1,0:T(8,128)(2,1)S(1)} %pack.2), channel_id=1, replica_groups=mesh['dp'=4,'z8'=8,'zp'=2,'y'=4,'tp'=2] {'zp','y'}, dimensions={0} | all-to-all | bytes 2228224 | tf_op jit(solution)/shard_map/cond/branch_0_fun/all_to_all | solution.py:292
  21.5 0.3 project.2
  21.8 29.6 %all_to_all.30 = bf16[8,8,1664]{2,1,0:T(8,128)(2,1)S(1)} all-to-all(bf16[8,8,1664]{2,1,0:T(8,128)(2,1)S(1)} %bitcast.18), channel_id=1, replica_groups=mesh['dp'=4,'z8'=8,'zp'=2,'y'=4,'tp'=2] {'z8'}, dimensions={0} | all-to-all | bytes 425984 | tf_op jit(solution)/shard_map/all_to_all | solution.py:292
  51.4 0.0 copy-done
  51.4 0.0 copy-done.2
  51.4 0.0 copy-done.3
  51.4 0.0 copy-done.4
  51.4 0.0 copy-done.5
  51.4 2.0 %delta.1 = (f32[2,4,8,4096]{3,2,1,0:T(8,128)S(1)}, bf16[64,512]{1,0:T(8,128)(2,1)S(1)}) custom-call(s32[2]{0:T(128)S(1)} %copy-done.3, bf16[64,1664]{1,0:T(8,128)(2,1)S(1)} %bitcast.12, f32[2,4,8,4096]{3,2,1,0:T(8,128)S(1)} %copy-done, f32[1,8]{1,0:T(1,128)S(1)} %bitcast.14, f32[2,4,8]{2,1,0:T(4,128)S(1)} %copy-done.2, f32[1,64]{1,0:T(1,128)S(1)} %bitcast.15), custom_call_target="tpu_custom_call" | custom-call | tf_op jit(solution)/shard_map/delta/pallas_call | solution.py:261
  53.5 0.0 copy-start.1
  53.5 16.8 %all_to_all.31 = bf16[8,8,512]{2,1,0:T(8,128)(2,1)S(1)} all-to-all(bf16[8,8,512]{2,1,0:T(8,128)(2,1)S(1)} %bitcast.13), channel_id=1, replica_groups=mesh['dp'=4,'z8'=8,'zp'=2,'y'=4,'tp'=2] {'z8'}, dimensions={0} | all-to-all | bytes 131072 | tf_op jit(solution)/shard_map/all_to_all | solution.py:292
  70.2 0.2 conditional.3
  70.2 0.2 mix.2
  70.5 12.0 %all_to_all.32.x_ref = bf16[16,16,128]{2,1,0:T(8,128)(2,1)S(1)} all-to-all(bf16[16,16,128]{2,1,0:T(8,128)(2,1)S(1)} %get-tuple-element.84), channel_id=1, replica_groups=mesh['dp'=4,'z8'=8,'zp'=2,'y'=4,'tp'=2] {'zp','y','tp'}, dimensions={0} | all-to-all | bytes 131072 | tf_op jit(solution)/shard_map/all_to_all | solution.py:292
  82.5 0.0 copy-done.1
  82.5 1.7 %place.1 = (bf16[4,32,128]{2,1,0:T(8,128)(2,1)}, f32[2,4,8,4096]{3,2,1,0:T(8,128)}) custom-call(bf16[16,16,128]{2,1,0:T(8,128)(2,1)S(1)} %all_to_all.32.x_ref, bf16[512,512]{1,0:T(8,128)(2,1)S(1)} %copy-done.1, f32[2,4,8,4096]{3,2,1,0:T(8,128)S(1)} %get-tuple-element.76.states_ref), custom_call_target="tpu_custom_call" | custom-call | tf_op jit(solution)/shard_map/place/pallas_call | solution.py:261
Async XLA Ops:
  0.6 50.8 %copy-start = (f32[2,4,8,4096]{3,2,1,0:T(8,128)S(1)}, f32[2,4,8,4096]{3,2,1,0:T(8,128)}, u32[]{:S(2)}) copy-start(f32[2,4,8,4096]{3,2,1,0:T(8,128)} %prior_ref.1) | copy-start | bytes 3145732
  0.7 50.8 %copy-start.2 = (f32[2,4,8]{2,1,0:T(4,128)S(1)}, f32[2,4,8]{2,1,0:T(4,128)}, u32[]{:S(2)}) copy-start(f32[2,4,8]{2,1,0:T(4,128)} %extra_ref.1) | copy-start | bytes 772
  0.7 50.8 %copy-start.3 = (s32[2]{0:T(128)S(1)}, s32[2]{0:T(128)}, u32[]{:S(2)}) copy-start(s32[2]{0:T(128)} %accepted_ref.1) | copy-start | bytes 28
  0.7 50.7 %copy-start.4 = (f32[8]{0:T(128)S(1)}, f32[8]{0:T(128)}, u32[]{:S(2)}) copy-start(f32[8]{0:T(128)} %param.25) | copy-start | bytes 100
  0.7 50.7 %copy-start.5 = (f32[64]{0:T(128)S(1)}, f32[64]{0:T(128)}, u32[]{:S(2)}) copy-start(f32[64]{0:T(128)} %param.29) | copy-start | bytes 772
  53.5 29.1 %copy-start.1 = (bf16[512,512]{1,0:T(8,128)(2,1)S(1)}, bf16[512,512]{1,0:T(8,128)(2,1)}, u32[]{:S(2)}) copy-start(bf16[512,512]{1,0:T(8,128)(2,1)} %constant.12.clone.back_ref) | copy-start | bytes 1572868

commit v9 on v8

--- a/solution.py
+++ b/solution.py
@@ -48,24 +48,23 @@
     for copy in copies:
         copy.wait()
     gain = jnp.sum(jnp.where(eye, gain_ref[...], 0.0), axis=1, keepdims=True)
-    raw = jnp.concatenate([tok_ref[t] for t in range(4)], axis=1).astype(f32)
+    raw = dot(jnp.concatenate([tok_ref[t] for t in range(4)], axis=1), pick, 1, 0)
     scaled = raw * gain
     squares = jnp.sum(raw * raw, axis=0, keepdims=True)
     high = squares.astype(bf16).astype(f32)
-    sub = iota((16, 512), 0)
+    sub = iota((8, 512), 0)
     extra = jnp.where(sub < 2, high, jnp.where(sub < 4, squares - high, 0.0))
-    moved = dot(jnp.concatenate([scaled, extra], axis=0).astype(bf16), pick, 1, 0)
     small = dot(beta_ref[...], put_beta, 0, 0) + dot(decay_ref[...], put_decay, 0, 0)
     lane = iota((8, 128), 1)
     even = iota((8, 128), 0) % 2 == 0
     for r in range(8):
         at = slice(128 * (r // 2), 128 * (r // 2) + 128)
-        sums = moved[32:40, at]
+        sums = extra[:, at]
         if r % 2 == 0:
-            cols = pltpu.roll(moved[:32, at], 64, 1)
+            cols = pltpu.roll(scaled[:, at], 64, 1)
             sums = jnp.where(even, pltpu.roll(sums, 32, 1), sums)
         else:
-            cols = moved[:32, at]
+            cols = scaled[:, at]
             sums = jnp.where(even, pltpu.roll(sums, 96, 1), pltpu.roll(sums, 64, 1))
         groups = []
         for g in range(4):
@@ -107,7 +106,7 @@
 
 def delta_kernel(
     accepted_ref, c_ref, prior_ref, rate_ref, extra_ref, gain_ref, states_ref, rows_ref,
-    aux, nrows, kept
+    aux, nrows, spread_ref
 ):
     c = c_ref[...].astype(f32)
     s = (c[0:8] + c[8:16]) + (c[16:24] + c[24:32])
@@ -144,36 +143,51 @@
     def half_sum(values):
         return 0.5 * jnp.sum(values, axis=1, keepdims=True)
 
-    def unit(values):
-        return values * lax.rsqrt(half_sum(values * values) + epsilon)
+    def norm(values):
+        return lax.rsqrt(half_sum(values * values) + epsilon)
 
     ROWS = range(8)
-    q = [unit(by_heads(parts[0], row)) * 0.125 for row in ROWS]
-    k = [unit(by_heads(parts[1], row)) for row in ROWS]
+    q = [by_heads(parts[0], row) for row in ROWS]
+    k = [by_heads(parts[1], row) for row in ROWS]
     v = [by_heads(parts[2], row) for row in ROWS]
+    q_norm = [norm(values) * 0.125 for values in q]
+    k_norm = [norm(values) for values in k]
     a = [jnp.broadcast_to(fade[:, row : row + 1], (8, 128)) for row in ROWS]
     b = [jnp.broadcast_to(beta[:, row : row + 1], (8, 128)) for row in ROWS]
+
+    tall = jnp.concatenate(q + k, axis=0)
+    first = tall.astype(bf16).astype(f32)
+    second = (tall - first).astype(bf16).astype(f32)
+    left = iota(tall.shape, 1) < 64
+    one = jnp.where(left, first, second).astype(bf16)
+    two = jnp.where(left, tall - first - second, 0.0).astype(bf16)
+    bit, column = iota((256, 256), 0), iota((256, 256), 1)
+    wide = (bit % 64 == column // 64).astype(f32).astype(bf16)
+    for n in range(16):
+        if n > 0:
+            turned = [pltpu.roll(half, 128 - 4 * n, 1) for half in (one, two)]
+        else:
+            turned = [one, two]
+        spread_ref[:, 256 * n : 256 * n + 256] = dot(jnp.concatenate(turned, axis=1), wide, 1, 0)
 
     starts = [accepted_ref[0] - 1, accepted_ref[1] - 1]
     ks, qs = [None] * 8, [None] * 8
     for i in range(32):
-        index = lane // 64 + 2 * i
         at = slice(128 * i, 128 * i + 128)
         for j in range(2):
             start = prior_ref[j, starts[j], :, at]
             for row in range(4 * j, 4 * j + 4):
-                kx = jnp.take_along_axis(k[row], index, axis=1, mode="promise_in_bounds")
-                qx = jnp.take_along_axis(q[row], index, axis=1, mode="promise_in_bounds")
-                kept[row, :, at] = kx
+                kx = spread_ref[64 + 8 * row : 72 + 8 * row, at]
+                qx = spread_ref[8 * row : 8 * row + 8, at]
                 ks[row] = kx * start if i == 0 else ks[row] + kx * start
                 qs[row] = qx * start if i == 0 else qs[row] + qx * start
 
     def fold(values):
         return values + pltpu.roll(values, 64, 1)
 
-    ks = [fold(values) for values in ks]
-    qs = [fold(values) for values in qs]
-    w, o = [None] * 8, [None] * 8
+    ks = [k_norm[row] * fold(ks[row]) for row in ROWS]
+    qs = [q_norm[row] * fold(qs[row]) for row in ROWS]
+    kw, o = [None] * 8, [None] * 8
     for j in range(2):
         base = 4 * j
         grown = None
@@ -181,18 +195,18 @@
             row = base + t
             carried = ks[row] if t == 0 else grown * ks[row]
             for e in range(t):
-                reach = half_sum(k[row] * k[base + e])
+                reach = half_sum(k[row] * k[base + e]) * k_norm[row]
                 for m in range(e + 1, t):
                     reach = reach * a[base + m]
-                carried = carried + reach * w[base + e]
-            w[row] = b[row] * (v[row] - a[row] * carried)
+                carried = carried + reach * kw[base + e]
+            kw[row] = k_norm[row] * (b[row] * (v[row] - a[row] * carried))
             grown = a[row] if t == 0 else grown * a[row]
-            out = grown * qs[row] + half_sum(q[row] * k[row]) * w[row]
-            for e in range(t):
-                reach = half_sum(q[row] * k[base + e])
+            out = grown * qs[row]
+            for e in range(t + 1):
+                reach = half_sum(q[row] * k[base + e]) * q_norm[row]
                 for m in range(e + 1, t + 1):
                     reach = reach * a[base + m]
-                out = out + reach * w[base + e]
+                out = out + reach * kw[base + e]
             o[row] = out
 
     for j in range(2):
@@ -201,7 +215,7 @@
             state = prior_ref[j, starts[j], :, at]
             for t in range(4):
                 row = 4 * j + t
-                state = a[row] * state + kept[row, :, at] * w[row]
+                state = a[row] * state + spread_ref[64 + 8 * row : 72 + 8 * row, at] * kw[row]
                 states_ref[j, t, :, at] = state
 
     for row in ROWS:
@@ -359,7 +373,7 @@
         scratch=[
             pltpu.VMEM((8, 128), f32),
             pltpu.VMEM((8, 512), f32),
-            pltpu.VMEM((8, 8, 4096), f32),
+            pltpu.VMEM((128, 4096), f32),
         ],
         outs=(VMEM, VMEM),
         name="delta",

time: 84.5 us -> 84.2 us (level)
  no operation moved by 1% of the time
where the time goes in v9:
time: 84.2 us; the launch traced here: 83.9 us
  blocking collectives  77.8 us (92%)
  Pallas kernels  5.27 us (6%)
    all_to_all x4, blocking collectives, swap(): return lax.all_to_all(x, axes, 0, 0, tiled=True)  77.8 us
    pallas_call x5, Pallas kernels, call(): pl.pallas_call(kernel, out_shape=shapes, in_specs=specs or [VMEM] * len(a...  5.27 us

profile of v9, /device:TPU:1, one launch (start us, length us, event | category | flops | bytes accessed | tf_op | source)
XLA Modules:
  0.0 83.9 jit_solution(8901050632379690284)
XLA Ops:
  0.6 0.0 copy-start
  0.7 0.0 copy-start.2
  0.7 0.0 copy-start.3
  0.7 0.0 copy-start.4
  0.7 0.0 copy-start.5
  0.7 21.1 %conditional.2 = ((bf16[64,1664]{1,0:T(8,128)(2,1)S(1)}, bf16[8,32,512]{2,1,0:T(8,128)(2,1)S(1)})) conditional(s32[]{:T(128)} %convert_element_type.4, (bf16[4,32,128]{2,1,0:T(8,128)(2,1)}, f32[1,32]{1,0:T(1,128)}, bf16[32,512]{1,0:T(8,128)(2,1)}, bf16[32,512]{1,0:T(8,128)(2,1)}, bf16[32,512]{1,0:T(8,128)(2,1)}, /*index=5*/bf16[8,32]{1,0:T(8,128)(2,1)}, ...), branch_computations={%region_0.0_spmd, %region_1.0_spmd} | conditional | bytes 2228232 | solution.py:347
  0.7 1.3 %pack.2 = bf16[8,32,2176]{2,1,0:T(8,128)(2,1)S(1)} custom-call(bf16[4,32,128]{2,1,0:T(8,128)(2,1)} %get-tuple-element.40.refs_0_, f32[1,32]{1,0:T(1,128)} %get-tuple-element.44.refs_1_, bf16[32,512]{1,0:T(8,128)(2,1)} %get-tuple-element.45.refs_2_, bf16[32,512]{1,0:T(8,128)(2,1)} %get-tuple-element.46.refs_3_, bf16[32,512]{1,0:T(8,128)(2,1)} %get-tuple-element.47.refs_4_, ...), custom_call_target="tpu_custom_call" | custom-call | tf_op jit(solution)/shard_map/cond/branch_0_fun/pack/pallas_call | solution.py:275
  2.1 19.4 %all_to_all.27.x_ref = bf16[8,32,2176]{2,1,0:T(8,128)(2,1)S(1)} all-to-all(bf16[8,32,2176]{2,1,0:T(8,128)(2,1)S(1)} %pack.2), channel_id=1, replica_groups=mesh['dp'=4,'z8'=8,'zp'=2,'y'=4,'tp'=2] {'zp','y'}, dimensions={0} | all-to-all | bytes 2228224 | tf_op jit(solution)/shard_map/cond/branch_0_fun/all_to_all | solution.py:306
  21.5 0.3 project.2
  21.8 29.6 %all_to_all.30 = bf16[8,8,1664]{2,1,0:T(8,128)(2,1)S(1)} all-to-all(bf16[8,8,1664]{2,1,0:T(8,128)(2,1)S(1)} %bitcast.18), channel_id=1, replica_groups=mesh['dp'=4,'z8'=8,'zp'=2,'y'=4,'tp'=2] {'z8'}, dimensions={0} | all-to-all | bytes 425984 | tf_op jit(solution)/shard_map/all_to_all | solution.py:306
  51.4 0.0 copy-done
  51.4 0.0 copy-done.2
  51.4 0.0 copy-done.3
  51.4 0.0 copy-done.4
  51.4 0.0 copy-done.5
  51.4 1.7 %delta.1 = (f32[2,4,8,4096]{3,2,1,0:T(8,128)S(1)}, bf16[64,512]{1,0:T(8,128)(2,1)S(1)}) custom-call(s32[2]{0:T(128)S(1)} %copy-done.3, bf16[64,1664]{1,0:T(8,128)(2,1)S(1)} %bitcast.12, f32[2,4,8,4096]{3,2,1,0:T(8,128)S(1)} %copy-done, f32[1,8]{1,0:T(1,128)S(1)} %bitcast.14, f32[2,4,8]{2,1,0:T(4,128)S(1)} %copy-done.2, f32[1,64]{1,0:T(1,128)S(1)} %bitcast.15), custom_call_target="tpu_custom_call" | custom-call | tf_op jit(solution)/shard_map/delta/pallas_call | solution.py:275
  53.1 0.0 copy-start.1
  53.2 16.8 %all_to_all.31 = bf16[8,8,512]{2,1,0:T(8,128)(2,1)S(1)} all-to-all(bf16[8,8,512]{2,1,0:T(8,128)(2,1)S(1)} %bitcast.13), channel_id=1, replica_groups=mesh['dp'=4,'z8'=8,'zp'=2,'y'=4,'tp'=2] {'z8'}, dimensions={0} | all-to-all | bytes 131072 | tf_op jit(solution)/shard_map/all_to_all | solution.py:306
  69.9 0.2 conditional.3
  69.9 0.2 mix.2
  70.2 12.1 %all_to_all.32.x_ref = bf16[16,16,128]{2,1,0:T(8,128)(2,1)S(1)} all-to-all(bf16[16,16,128]{2,1,0:T(8,128)(2,1)S(1)} %get-tuple-element.84), channel_id=1, replica_groups=mesh['dp'=4,'z8'=8,'zp'=2,'y'=4,'tp'=2] {'zp','y','tp'}, dimensions={0} | all-to-all | bytes 131072 | tf_op jit(solution)/shard_map/all_to_all | solution.py:306
  82.2 0.0 copy-done.1
  82.2 1.7 %place.1 = (bf16[4,32,128]{2,1,0:T(8,128)(2,1)}, f32[2,4,8,4096]{3,2,1,0:T(8,128)}) custom-call(bf16[16,16,128]{2,1,0:T(8,128)(2,1)S(1)} %all_to_all.32.x_ref, bf16[512,512]{1,0:T(8,128)(2,1)S(1)} %copy-done.1, f32[2,4,8,4096]{3,2,1,0:T(8,128)S(1)} %get-tuple-element.76.states_ref), custom_call_target="tpu_custom_call" | custom-call | tf_op jit(solution)/shard_map/place/pallas_call | solution.py:275
Async XLA Ops:
  0.6 50.8 %copy-start = (f32[2,4,8,4096]{3,2,1,0:T(8,128)S(1)}, f32[2,4,8,4096]{3,2,1,0:T(8,128)}, u32[]{:S(2)}) copy-start(f32[2,4,8,4096]{3,2,1,0:T(8,128)} %prior_ref.1) | copy-start | bytes 3145732
  0.7 50.8 %copy-start.2 = (f32[2,4,8]{2,1,0:T(4,128)S(1)}, f32[2,4,8]{2,1,0:T(4,128)}, u32[]{:S(2)}) copy-start(f32[2,4,8]{2,1,0:T(4,128)} %extra_ref.1) | copy-start | bytes 772
  0.7 50.8 %copy-start.3 = (s32[2]{0:T(128)S(1)}, s32[2]{0:T(128)}, u32[]{:S(2)}) copy-start(s32[2]{0:T(128)} %accepted_ref.1) | copy-start | bytes 28
  0.7 50.7 %copy-start.4 = (f32[8]{0:T(128)S(1)}, f32[8]{0:T(128)}, u32[]{:S(2)}) copy-start(f32[8]{0:T(128)} %param.25) | copy-start | bytes 100
  0.7 50.7 %copy-start.5 = (f32[64]{0:T(128)S(1)}, f32[64]{0:T(128)}, u32[]{:S(2)}) copy-start(f32[64]{0:T(128)} %param.29) | copy-start | bytes 772
  53.1 29.1 %copy-start.1 = (bf16[512,512]{1,0:T(8,128)(2,1)S(1)}, bf16[512,512]{1,0:T(8,128)(2,1)}, u32[]{:S(2)}) copy-start(bf16[512,512]{1,0:T(8,128)(2,1)} %constant.12.clone.back_ref) | copy-start | bytes 1572868

commit v10 on v9

--- a/solution.py
+++ b/solution.py
@@ -343,7 +343,7 @@
         return call(mix_kernel, shape((16, 16, 128), bf16), (weights, rows), name="mix")
 
     pair = lax.axis_index("z8")
-    late = (pair >= 4) & (pair <= 6)
+    late = pair >= 3
     part, weights = lax.cond(
         late,
         start_late,

time: 84.2 us -> 84.2 us (level)
  no operation moved by 1% of the time
where the time goes in v10:
time: 84.2 us; the launch traced here: 83.9 us
  blocking collectives  77.8 us (92%)
  Pallas kernels  5.28 us (6%)
    all_to_all x4, blocking collectives, swap(): return lax.all_to_all(x, axes, 0, 0, tiled=True)  77.8 us
    pallas_call x5, Pallas kernels, call(): pl.pallas_call(kernel, out_shape=shapes, in_specs=specs or [VMEM] * len(a...  5.28 us

profile of v10, /device:TPU:1, one launch (start us, length us, event | category | flops | bytes accessed | tf_op | source)
XLA Modules:
  0.0 83.9 jit_solution(8370436034274472211)
XLA Ops:
  0.6 0.0 copy-start
  0.6 0.0 copy-start.2
  0.7 0.0 copy-start.3
  0.7 0.0 copy-start.4
  0.7 0.0 copy-start.5
  0.7 21.1 %conditional.2 = ((bf16[64,1664]{1,0:T(8,128)(2,1)S(1)}, bf16[8,32,512]{2,1,0:T(8,128)(2,1)S(1)})) conditional(s32[]{:T(128)} %convert_element_type.4, (bf16[4,32,128]{2,1,0:T(8,128)(2,1)}, f32[1,32]{1,0:T(1,128)}, bf16[32,512]{1,0:T(8,128)(2,1)}, bf16[32,512]{1,0:T(8,128)(2,1)}, bf16[32,512]{1,0:T(8,128)(2,1)}, /*index=5*/bf16[8,32]{1,0:T(8,128)(2,1)}, ...), branch_computations={%region_0.0_spmd, %region_1.0_spmd} | conditional | bytes 2228232 | solution.py:347
  0.7 1.3 %pack.2 = bf16[8,32,2176]{2,1,0:T(8,128)(2,1)S(1)} custom-call(bf16[4,32,128]{2,1,0:T(8,128)(2,1)} %get-tuple-element.40.refs_0_, f32[1,32]{1,0:T(1,128)} %get-tuple-element.44.refs_1_, bf16[32,512]{1,0:T(8,128)(2,1)} %get-tuple-element.45.refs_2_, bf16[32,512]{1,0:T(8,128)(2,1)} %get-tuple-element.46.refs_3_, bf16[32,512]{1,0:T(8,128)(2,1)} %get-tuple-element.47.refs_4_, ...), custom_call_target="tpu_custom_call" | custom-call | tf_op jit(solution)/shard_map/cond/branch_0_fun/pack/pallas_call | solution.py:275
  2.1 19.4 %all_to_all.27.x_ref = bf16[8,32,2176]{2,1,0:T(8,128)(2,1)S(1)} all-to-all(bf16[8,32,2176]{2,1,0:T(8,128)(2,1)S(1)} %pack.2), channel_id=1, replica_groups=mesh['dp'=4,'z8'=8,'zp'=2,'y'=4,'tp'=2] {'zp','y'}, dimensions={0} | all-to-all | bytes 2228224 | tf_op jit(solution)/shard_map/cond/branch_0_fun/all_to_all | solution.py:306
  21.5 0.3 project.2
  21.8 29.6 %all_to_all.30 = bf16[8,8,1664]{2,1,0:T(8,128)(2,1)S(1)} all-to-all(bf16[8,8,1664]{2,1,0:T(8,128)(2,1)S(1)} %bitcast.18), channel_id=1, replica_groups=mesh['dp'=4,'z8'=8,'zp'=2,'y'=4,'tp'=2] {'z8'}, dimensions={0} | all-to-all | bytes 425984 | tf_op jit(solution)/shard_map/all_to_all | solution.py:306
  51.4 0.0 copy-done
  51.4 0.0 copy-done.2
  51.4 0.0 copy-done.3
  51.4 0.0 copy-done.4
  51.4 0.0 copy-done.5
  51.4 1.7 %delta.1 = (f32[2,4,8,4096]{3,2,1,0:T(8,128)S(1)}, bf16[64,512]{1,0:T(8,128)(2,1)S(1)}) custom-call(s32[2]{0:T(128)S(1)} %copy-done.3, bf16[64,1664]{1,0:T(8,128)(2,1)S(1)} %bitcast.12, f32[2,4,8,4096]{3,2,1,0:T(8,128)S(1)} %copy-done, f32[1,8]{1,0:T(1,128)S(1)} %bitcast.14, f32[2,4,8]{2,1,0:T(4,128)S(1)} %copy-done.2, f32[1,64]{1,0:T(1,128)S(1)} %bitcast.15), custom_call_target="tpu_custom_call" | custom-call | tf_op jit(solution)/shard_map/delta/pallas_call | solution.py:275
  53.1 0.0 copy-start.1
  53.1 16.8 %all_to_all.31 = bf16[8,8,512]{2,1,0:T(8,128)(2,1)S(1)} all-to-all(bf16[8,8,512]{2,1,0:T(8,128)(2,1)S(1)} %bitcast.13), channel_id=1, replica_groups=mesh['dp'=4,'z8'=8,'zp'=2,'y'=4,'tp'=2] {'z8'}, dimensions={0} | all-to-all | bytes 131072 | tf_op jit(solution)/shard_map/all_to_all | solution.py:306
  69.9 0.2 conditional.3
  69.9 0.2 mix.2
  70.2 12.0 %all_to_all.32.x_ref = bf16[16,16,128]{2,1,0:T(8,128)(2,1)S(1)} all-to-all(bf16[16,16,128]{2,1,0:T(8,128)(2,1)S(1)} %get-tuple-element.84), channel_id=1, replica_groups=mesh['dp'=4,'z8'=8,'zp'=2,'y'=4,'tp'=2] {'zp','y','tp'}, dimensions={0} | all-to-all | bytes 131072 | tf_op jit(solution)/shard_map/all_to_all | solution.py:306
  82.2 0.0 copy-done.1
  82.2 1.7 %place.1 = (bf16[4,32,128]{2,1,0:T(8,128)(2,1)}, f32[2,4,8,4096]{3,2,1,0:T(8,128)}) custom-call(bf16[16,16,128]{2,1,0:T(8,128)(2,1)S(1)} %all_to_all.32.x_ref, bf16[512,512]{1,0:T(8,128)(2,1)S(1)} %copy-done.1, f32[2,4,8,4096]{3,2,1,0:T(8,128)S(1)} %get-tuple-element.76.states_ref), custom_call_target="tpu_custom_call" | custom-call | tf_op jit(solution)/shard_map/place/pallas_call | solution.py:275
Async XLA Ops:
  0.6 50.7 %copy-start = (f32[2,4,8,4096]{3,2,1,0:T(8,128)S(1)}, f32[2,4,8,4096]{3,2,1,0:T(8,128)}, u32[]{:S(2)}) copy-start(f32[2,4,8,4096]{3,2,1,0:T(8,128)} %prior_ref.1) | copy-start | bytes 3145732
  0.6 50.7 %copy-start.2 = (f32[2,4,8]{2,1,0:T(4,128)S(1)}, f32[2,4,8]{2,1,0:T(4,128)}, u32[]{:S(2)}) copy-start(f32[2,4,8]{2,1,0:T(4,128)} %extra_ref.1) | copy-start | bytes 772
  0.7 50.7 %copy-start.3 = (s32[2]{0:T(128)S(1)}, s32[2]{0:T(128)}, u32[]{:S(2)}) copy-start(s32[2]{0:T(128)} %accepted_ref.1) | copy-start | bytes 28
  0.7 50.7 %copy-start.4 = (f32[8]{0:T(128)S(1)}, f32[8]{0:T(128)}, u32[]{:S(2)}) copy-start(f32[8]{0:T(128)} %param.25) | copy-start | bytes 100
  0.7 50.7 %copy-start.5 = (f32[64]{0:T(128)S(1)}, f32[64]{0:T(128)}, u32[]{:S(2)}) copy-start(f32[64]{0:T(128)} %param.29) | copy-start | bytes 772
  53.1 29.1 %copy-start.1 = (bf16[512,512]{1,0:T(8,128)(2,1)S(1)}, bf16[512,512]{1,0:T(8,128)(2,1)}, u32[]{:S(2)}) copy-start(bf16[512,512]{1,0:T(8,128)(2,1)} %constant.10.clone.back_ref) | copy-start | bytes 1572868

commit v11 on v9

--- a/solution.py
+++ b/solution.py
@@ -13,7 +13,7 @@
 epsilon = 1e-06
 KV = ("z8", "zp", "y")
 DP_KV = ("dp", "z8", "zp", "y")
-NEAR = ("zp", "y")
+NEAR = ("y", "zp")
 f32 = jnp.float32
 bf16 = jnp.bfloat16
 
@@ -39,6 +39,7 @@
     tok_ref, gain_ref, q_ref, k_ref, v_ref, beta_ref, decay_ref, wo_ref = held
     source, dest = iota((512, 512), 0), iota((1, 512), 1)
     group, rho = dest // 64, dest % 64
+    group = (group % 2) * 4 + group // 2
     wanted = (rho % 4) * 128 + (rho // 8) * 16 + group * 2 + (rho % 8) // 4
     pick = (source == wanted).astype(f32).astype(bf16)
     eye = iota((32, 32), 0) == iota((32, 32), 1)
@@ -265,6 +266,7 @@
 def back_table():
     dest = np.arange(512)
     group, rho = dest // 64, dest % 64
+    group = (group % 2) * 4 + group // 2
     wanted = (rho % 4) * 128 + (rho // 8) * 16 + group * 2 + (rho % 8) // 4
     return (wanted[:, None] == np.arange(512)[None, :]).astype(jnp.bfloat16)
 
@@ -382,7 +384,7 @@
     columns = lax.cond(
         late, lambda w, r: mix(swap(w, NEAR), r), lambda w, r: mix(w, r), weights, all_rows
     )
-    back = swap(columns, ("zp", "y", "tp"))
+    back = swap(columns, ("y", "zp", "tp"))
     mixed, kept = call(
         place_kernel,
         (shape((4, 32, 128), bf16), shape(states.shape, f32)),

time: 84.2 us -> 84 us (level)
  no operation moved by 1% of the time
where the time goes in v11:
time: 84 us; the launch traced here: 83.7 us
  blocking collectives  77.7 us (92%)
  Pallas kernels  5.27 us (6%)
    all_to_all x4, blocking collectives, swap(): return lax.all_to_all(x, axes, 0, 0, tiled=True)  77.7 us
    pallas_call x5, Pallas kernels, call(): pl.pallas_call(kernel, out_shape=shapes, in_specs=specs or [VMEM] * len(a...  5.27 us

profile of v11, /device:TPU:1, one launch (start us, length us, event | category | flops | bytes accessed | tf_op | source)
XLA Modules:
  0.0 83.7 jit_solution(14320264803084558779)
XLA Ops:
  0.6 0.0 copy-start
  0.7 0.0 copy-start.2
  0.7 0.0 copy-start.3
  0.7 0.0 copy-start.4
  0.7 0.0 copy-start.5
  0.7 21.3 %conditional.2 = ((bf16[64,1664]{1,0:T(8,128)(2,1)S(1)}, bf16[8,32,512]{2,1,0:T(8,128)(2,1)S(1)})) conditional(s32[]{:T(128)} %convert_element_type.4, (bf16[4,32,128]{2,1,0:T(8,128)(2,1)}, f32[1,32]{1,0:T(1,128)}, bf16[32,512]{1,0:T(8,128)(2,1)}, bf16[32,512]{1,0:T(8,128)(2,1)}, bf16[32,512]{1,0:T(8,128)(2,1)}, /*index=5*/bf16[8,32]{1,0:T(8,128)(2,1)}, ...), branch_computations={%region_0.0_spmd, %region_1.0_spmd} | conditional | bytes 2228232 | solution.py:349
  0.7 1.3 %pack.2 = bf16[8,32,2176]{2,1,0:T(8,128)(2,1)S(1)} custom-call(bf16[4,32,128]{2,1,0:T(8,128)(2,1)} %get-tuple-element.40.refs_0_, f32[1,32]{1,0:T(1,128)} %get-tuple-element.44.refs_1_, bf16[32,512]{1,0:T(8,128)(2,1)} %get-tuple-element.45.refs_2_, bf16[32,512]{1,0:T(8,128)(2,1)} %get-tuple-element.46.refs_3_, bf16[32,512]{1,0:T(8,128)(2,1)} %get-tuple-element.47.refs_4_, ...), custom_call_target="tpu_custom_call" | custom-call | tf_op jit(solution)/shard_map/cond/branch_0_fun/pack/pallas_call | solution.py:277
  2.1 19.6 %all_to_all.27.x_ref = bf16[8,32,2176]{2,1,0:T(8,128)(2,1)S(1)} all-to-all(bf16[8,32,2176]{2,1,0:T(8,128)(2,1)S(1)} %pack.2), channel_id=1, replica_groups=mesh['dp'=4,'z8'=8,'zp'=2,'y'=4,'tp'=2] {'y','zp'}, dimensions={0} | all-to-all | bytes 2228224 | tf_op jit(solution)/shard_map/cond/branch_0_fun/all_to_all | solution.py:308
  21.6 0.3 project.2
  22.0 29.6 %all_to_all.30 = bf16[8,8,1664]{2,1,0:T(8,128)(2,1)S(1)} all-to-all(bf16[8,8,1664]{2,1,0:T(8,128)(2,1)S(1)} %bitcast.18), channel_id=1, replica_groups=mesh['dp'=4,'z8'=8,'zp'=2,'y'=4,'tp'=2] {'z8'}, dimensions={0} | all-to-all | bytes 425984 | tf_op jit(solution)/shard_map/all_to_all | solution.py:308
  51.5 0.0 copy-done
  51.5 0.0 copy-done.2
  51.5 0.0 copy-done.3
  51.5 0.0 copy-done.4
  51.6 0.0 copy-done.5
  51.6 1.7 %delta.1 = (f32[2,4,8,4096]{3,2,1,0:T(8,128)S(1)}, bf16[64,512]{1,0:T(8,128)(2,1)S(1)}) custom-call(s32[2]{0:T(128)S(1)} %copy-done.3, bf16[64,1664]{1,0:T(8,128)(2,1)S(1)} %bitcast.12, f32[2,4,8,4096]{3,2,1,0:T(8,128)S(1)} %copy-done, f32[1,8]{1,0:T(1,128)S(1)} %bitcast.14, f32[2,4,8]{2,1,0:T(4,128)S(1)} %copy-done.2, f32[1,64]{1,0:T(1,128)S(1)} %bitcast.15), custom_call_target="tpu_custom_call" | custom-call | tf_op jit(solution)/shard_map/delta/pallas_call | solution.py:277
  53.3 0.0 copy-start.1
  53.3 16.8 %all_to_all.31 = bf16[8,8,512]{2,1,0:T(8,128)(2,1)S(1)} all-to-all(bf16[8,8,512]{2,1,0:T(8,128)(2,1)S(1)} %bitcast.13), channel_id=1, replica_groups=mesh['dp'=4,'z8'=8,'zp'=2,'y'=4,'tp'=2] {'z8'}, dimensions={0} | all-to-all | bytes 131072 | tf_op jit(solution)/shard_map/all_to_all | solution.py:308
  70.0 0.2 conditional.3
  70.0 0.2 mix.2
  70.3 11.8 %all_to_all.32.x_ref = bf16[16,16,128]{2,1,0:T(8,128)(2,1)S(1)} all-to-all(bf16[16,16,128]{2,1,0:T(8,128)(2,1)S(1)} %get-tuple-element.84), channel_id=1, replica_groups=mesh['dp'=4,'z8'=8,'zp'=2,'y'=4,'tp'=2] {'y','zp','tp'}, dimensions={0} | all-to-all | bytes 131072 | tf_op jit(solution)/shard_map/all_to_all | solution.py:308
  82.1 0.0 copy-done.1
  82.1 1.7 %place.1 = (bf16[4,32,128]{2,1,0:T(8,128)(2,1)}, f32[2,4,8,4096]{3,2,1,0:T(8,128)}) custom-call(bf16[16,16,128]{2,1,0:T(8,128)(2,1)S(1)} %all_to_all.32.x_ref, bf16[512,512]{1,0:T(8,128)(2,1)S(1)} %copy-done.1, f32[2,4,8,4096]{3,2,1,0:T(8,128)S(1)} %get-tuple-element.76.states_ref), custom_call_target="tpu_custom_call" | custom-call | tf_op jit(solution)/shard_map/place/pallas_call | solution.py:277
Async XLA Ops:
  0.6 50.9 %copy-start = (f32[2,4,8,4096]{3,2,1,0:T(8,128)S(1)}, f32[2,4,8,4096]{3,2,1,0:T(8,128)}, u32[]{:S(2)}) copy-start(f32[2,4,8,4096]{3,2,1,0:T(8,128)} %prior_ref.1) | copy-start | bytes 3145732
  0.7 50.9 %copy-start.2 = (f32[2,4,8]{2,1,0:T(4,128)S(1)}, f32[2,4,8]{2,1,0:T(4,128)}, u32[]{:S(2)}) copy-start(f32[2,4,8]{2,1,0:T(4,128)} %extra_ref.1) | copy-start | bytes 772
  0.7 50.9 %copy-start.3 = (s32[2]{0:T(128)S(1)}, s32[2]{0:T(128)}, u32[]{:S(2)}) copy-start(s32[2]{0:T(128)} %accepted_ref.1) | copy-start | bytes 28
  0.7 50.9 %copy-start.4 = (f32[8]{0:T(128)S(1)}, f32[8]{0:T(128)}, u32[]{:S(2)}) copy-start(f32[8]{0:T(128)} %param.25) | copy-start | bytes 100
  0.7 50.9 %copy-start.5 = (f32[64]{0:T(128)S(1)}, f32[64]{0:T(128)}, u32[]{:S(2)}) copy-start(f32[64]{0:T(128)} %param.29) | copy-start | bytes 772
  53.3 28.8 %copy-start.1 = (bf16[512,512]{1,0:T(8,128)(2,1)S(1)}, bf16[512,512]{1,0:T(8,128)(2,1)}, u32[]{:S(2)}) copy-start(bf16[512,512]{1,0:T(8,128)(2,1)} %constant.12.clone.back_ref) | copy-start | bytes 1572868

commit v12 on v11

--- a/solution.py
+++ b/solution.py
@@ -237,19 +237,18 @@
     low = iota((16, 128), 1) < 64
     for r in range(8):
         piece = jnp.where(low, out[32 * r : 32 * r + 16], out[32 * r + 16 : 32 * r + 32])
-        out_ref[2 * r] = piece.astype(bf16)
-        out_ref[2 * r + 1] = piece.astype(bf16)
+        out_ref[r] = piece.astype(bf16)
+        out_ref[8 + r] = piece.astype(bf16)
 
 
 def place_kernel(x_ref, back_ref, states_ref, out_ref, kept_ref, sem):
     copies = [
-        pltpu.make_async_copy(states_ref.at[n // 4, n % 4], kept_ref.at[n // 4, n % 4], sem.at[n])
-        for n in range(8)
+        pltpu.make_async_copy(states_ref.at[n], kept_ref.at[n], sem.at[n]) for n in range(2)
     ]
     for copy in copies:
         copy.start()
     low = iota((16, 128), 1) < 64
-    sums = [x_ref[2 * r].astype(f32) + x_ref[2 * r + 1].astype(f32) for r in range(8)]
+    sums = [x_ref[r].astype(f32) + x_ref[8 + r].astype(f32) for r in range(8)]
     tiles = []
     for p in range(4):
         a, b = sums[2 * p], sums[2 * p + 1]
@@ -384,12 +383,12 @@
     columns = lax.cond(
         late, lambda w, r: mix(swap(w, NEAR), r), lambda w, r: mix(w, r), weights, all_rows
     )
-    back = swap(columns, ("y", "zp", "tp"))
+    back = swap(columns, ("tp", "y", "zp"))
     mixed, kept = call(
         place_kernel,
         (shape((4, 32, 128), bf16), shape(states.shape, f32)),
         (back, jnp.asarray(back_table()), states),
-        scratch=[pltpu.SemaphoreType.DMA((8,))],
+        scratch=[pltpu.SemaphoreType.DMA((2,))],
         outs=(VMEM, HBM),
         name="place",
     )

time: 84 us -> 83.7 us (level)
  no operation moved by 1% of the time
where the time goes in v12:
time: 83.7 us; the launch traced here: 83.5 us
  blocking collectives  77.4 us (92%)
  Pallas kernels  5.23 us (6%)
    all_to_all x4, blocking collectives, swap(): return lax.all_to_all(x, axes, 0, 0, tiled=True)  77.4 us
    pallas_call x5, Pallas kernels, call(): pl.pallas_call(kernel, out_shape=shapes, in_specs=specs or [VMEM] * len(a...  5.23 us

profile of v12, /device:TPU:1, one launch (start us, length us, event | category | flops | bytes accessed | tf_op | source)
XLA Modules:
  0.0 83.5 jit_solution(2049902288799269023)
XLA Ops:
  0.6 0.0 copy-start
  0.7 0.0 copy-start.2
  0.7 0.0 copy-start.3
  0.7 0.0 copy-start.4
  0.7 0.0 copy-start.5
  0.7 21.3 %conditional.2 = ((bf16[64,1664]{1,0:T(8,128)(2,1)S(1)}, bf16[8,32,512]{2,1,0:T(8,128)(2,1)S(1)})) conditional(s32[]{:T(128)} %convert_element_type.4, (bf16[4,32,128]{2,1,0:T(8,128)(2,1)}, f32[1,32]{1,0:T(1,128)}, bf16[32,512]{1,0:T(8,128)(2,1)}, bf16[32,512]{1,0:T(8,128)(2,1)}, bf16[32,512]{1,0:T(8,128)(2,1)}, /*index=5*/bf16[8,32]{1,0:T(8,128)(2,1)}, ...), branch_computations={%region_0.0_spmd, %region_1.0_spmd} | conditional | bytes 2228232 | solution.py:348
  0.7 1.3 %pack.2 = bf16[8,32,2176]{2,1,0:T(8,128)(2,1)S(1)} custom-call(bf16[4,32,128]{2,1,0:T(8,128)(2,1)} %get-tuple-element.40.refs_0_, f32[1,32]{1,0:T(1,128)} %get-tuple-element.44.refs_1_, bf16[32,512]{1,0:T(8,128)(2,1)} %get-tuple-element.45.refs_2_, bf16[32,512]{1,0:T(8,128)(2,1)} %get-tuple-element.46.refs_3_, bf16[32,512]{1,0:T(8,128)(2,1)} %get-tuple-element.47.refs_4_, ...), custom_call_target="tpu_custom_call" | custom-call | tf_op jit(solution)/shard_map/cond/branch_0_fun/pack/pallas_call | solution.py:276
  2.1 19.6 %all_to_all.27.x_ref = bf16[8,32,2176]{2,1,0:T(8,128)(2,1)S(1)} all-to-all(bf16[8,32,2176]{2,1,0:T(8,128)(2,1)S(1)} %pack.2), channel_id=1, replica_groups=mesh['dp'=4,'z8'=8,'zp'=2,'y'=4,'tp'=2] {'y','zp'}, dimensions={0} | all-to-all | bytes 2228224 | tf_op jit(solution)/shard_map/cond/branch_0_fun/all_to_all | solution.py:307
  21.6 0.3 project.2
  22.0 29.6 %all_to_all.30 = bf16[8,8,1664]{2,1,0:T(8,128)(2,1)S(1)} all-to-all(bf16[8,8,1664]{2,1,0:T(8,128)(2,1)S(1)} %bitcast.18), channel_id=1, replica_groups=mesh['dp'=4,'z8'=8,'zp'=2,'y'=4,'tp'=2] {'z8'}, dimensions={0} | all-to-all | bytes 425984 | tf_op jit(solution)/shard_map/all_to_all | solution.py:307
  51.5 0.0 copy-done
  51.5 0.0 copy-done.2
  51.5 0.0 copy-done.3
  51.5 0.0 copy-done.4
  51.6 0.0 copy-done.5
  51.6 1.7 %delta.1 = (f32[2,4,8,4096]{3,2,1,0:T(8,128)S(1)}, bf16[64,512]{1,0:T(8,128)(2,1)S(1)}) custom-call(s32[2]{0:T(128)S(1)} %copy-done.3, bf16[64,1664]{1,0:T(8,128)(2,1)S(1)} %bitcast.12, f32[2,4,8,4096]{3,2,1,0:T(8,128)S(1)} %copy-done, f32[1,8]{1,0:T(1,128)S(1)} %bitcast.14, f32[2,4,8]{2,1,0:T(4,128)S(1)} %copy-done.2, f32[1,64]{1,0:T(1,128)S(1)} %bitcast.15), custom_call_target="tpu_custom_call" | custom-call | tf_op jit(solution)/shard_map/delta/pallas_call | solution.py:276
  53.3 0.0 copy-start.1
  53.3 16.8 %all_to_all.31 = bf16[8,8,512]{2,1,0:T(8,128)(2,1)S(1)} all-to-all(bf16[8,8,512]{2,1,0:T(8,128)(2,1)S(1)} %bitcast.13), channel_id=1, replica_groups=mesh['dp'=4,'z8'=8,'zp'=2,'y'=4,'tp'=2] {'z8'}, dimensions={0} | all-to-all | bytes 131072 | tf_op jit(solution)/shard_map/all_to_all | solution.py:307
  70.0 0.2 conditional.3
  70.0 0.2 mix.2
  70.3 11.5 %all_to_all.32.x_ref = bf16[16,16,128]{2,1,0:T(8,128)(2,1)S(1)} all-to-all(bf16[16,16,128]{2,1,0:T(8,128)(2,1)S(1)} %get-tuple-element.84), channel_id=1, replica_groups=mesh['dp'=4,'z8'=8,'zp'=2,'y'=4,'tp'=2] {'tp','y','zp'}, dimensions={0} | all-to-all | bytes 131072 | tf_op jit(solution)/shard_map/all_to_all | solution.py:307
  81.8 0.0 copy-done.1
  81.8 1.6 %place.1 = (bf16[4,32,128]{2,1,0:T(8,128)(2,1)}, f32[2,4,8,4096]{3,2,1,0:T(8,128)}) custom-call(bf16[16,16,128]{2,1,0:T(8,128)(2,1)S(1)} %all_to_all.32.x_ref, bf16[512,512]{1,0:T(8,128)(2,1)S(1)} %copy-done.1, f32[2,4,8,4096]{3,2,1,0:T(8,128)S(1)} %get-tuple-element.76.states_ref), custom_call_target="tpu_custom_call" | custom-call | tf_op jit(solution)/shard_map/place/pallas_call | solution.py:276
Async XLA Ops:
  0.6 50.9 %copy-start = (f32[2,4,8,4096]{3,2,1,0:T(8,128)S(1)}, f32[2,4,8,4096]{3,2,1,0:T(8,128)}, u32[]{:S(2)}) copy-start(f32[2,4,8,4096]{3,2,1,0:T(8,128)} %prior_ref.1) | copy-start | bytes 3145732
  0.7 50.9 %copy-start.2 = (f32[2,4,8]{2,1,0:T(4,128)S(1)}, f32[2,4,8]{2,1,0:T(4,128)}, u32[]{:S(2)}) copy-start(f32[2,4,8]{2,1,0:T(4,128)} %extra_ref.1) | copy-start | bytes 772
  0.7 50.9 %copy-start.3 = (s32[2]{0:T(128)S(1)}, s32[2]{0:T(128)}, u32[]{:S(2)}) copy-start(s32[2]{0:T(128)} %accepted_ref.1) | copy-start | bytes 28
  0.7 50.9 %copy-start.4 = (f32[8]{0:T(128)S(1)}, f32[8]{0:T(128)}, u32[]{:S(2)}) copy-start(f32[8]{0:T(128)} %param.25) | copy-start | bytes 100
  0.7 50.9 %copy-start.5 = (f32[64]{0:T(128)S(1)}, f32[64]{0:T(128)}, u32[]{:S(2)}) copy-start(f32[64]{0:T(128)} %param.29) | copy-start | bytes 772
  53.3 28.5 %copy-start.1 = (bf16[512,512]{1,0:T(8,128)(2,1)S(1)}, bf16[512,512]{1,0:T(8,128)(2,1)}, u32[]{:S(2)}) copy-start(bf16[512,512]{1,0:T(8,128)(2,1)} %constant.12.clone.back_ref) | copy-start | bytes 1572868

commit v13 on v12

--- a/solution.py
+++ b/solution.py
@@ -243,7 +243,7 @@
 
 def place_kernel(x_ref, back_ref, states_ref, out_ref, kept_ref, sem):
     copies = [
-        pltpu.make_async_copy(states_ref.at[n], kept_ref.at[n], sem.at[n]) for n in range(2)
+        pltpu.make_async_copy(states_ref, kept_ref, sem.at[n]) for n in range(1)
     ]
     for copy in copies:
         copy.start()
@@ -388,7 +388,7 @@
         place_kernel,
         (shape((4, 32, 128), bf16), shape(states.shape, f32)),
         (back, jnp.asarray(back_table()), states),
-        scratch=[pltpu.SemaphoreType.DMA((2,))],
+        scratch=[pltpu.SemaphoreType.DMA((1,))],
         outs=(VMEM, HBM),
         name="place",
     )

time: 83.7 us -> 83.7 us (level)
  no operation moved by 1% of the time
where the time goes in v13:
time: 83.7 us; the launch traced here: 83.4 us
  blocking collectives  77.4 us (92%)
  Pallas kernels  5.22 us (6%)
    all_to_all x4, blocking collectives, swap(): return lax.all_to_all(x, axes, 0, 0, tiled=True)  77.4 us
    pallas_call x5, Pallas kernels, call(): pl.pallas_call(kernel, out_shape=shapes, in_specs=specs or [VMEM] * len(a...  5.22 us

profile of v13, /device:TPU:1, one launch (start us, length us, event | category | flops | bytes accessed | tf_op | source)
XLA Modules:
  0.0 83.4 jit_solution(2586987949674786618)
XLA Ops:
  0.6 0.0 copy-start
  0.7 0.0 copy-start.2
  0.7 0.0 copy-start.3
  0.7 0.0 copy-start.4
  0.7 0.0 copy-start.5
  0.7 21.3 %conditional.2 = ((bf16[64,1664]{1,0:T(8,128)(2,1)S(1)}, bf16[8,32,512]{2,1,0:T(8,128)(2,1)S(1)})) conditional(s32[]{:T(128)} %convert_element_type.4, (bf16[4,32,128]{2,1,0:T(8,128)(2,1)}, f32[1,32]{1,0:T(1,128)}, bf16[32,512]{1,0:T(8,128)(2,1)}, bf16[32,512]{1,0:T(8,128)(2,1)}, bf16[32,512]{1,0:T(8,128)(2,1)}, /*index=5*/bf16[8,32]{1,0:T(8,128)(2,1)}, ...), branch_computations={%region_0.0_spmd, %region_1.0_spmd} | conditional | bytes 2228232 | solution.py:348
  0.7 1.3 %pack.2 = bf16[8,32,2176]{2,1,0:T(8,128)(2,1)S(1)} custom-call(bf16[4,32,128]{2,1,0:T(8,128)(2,1)} %get-tuple-element.40.refs_0_, f32[1,32]{1,0:T(1,128)} %get-tuple-element.44.refs_1_, bf16[32,512]{1,0:T(8,128)(2,1)} %get-tuple-element.45.refs_2_, bf16[32,512]{1,0:T(8,128)(2,1)} %get-tuple-element.46.refs_3_, bf16[32,512]{1,0:T(8,128)(2,1)} %get-tuple-element.47.refs_4_, ...), custom_call_target="tpu_custom_call" | custom-call | tf_op jit(solution)/shard_map/cond/branch_0_fun/pack/pallas_call | solution.py:276
  2.1 19.6 %all_to_all.27.x_ref = bf16[8,32,2176]{2,1,0:T(8,128)(2,1)S(1)} all-to-all(bf16[8,32,2176]{2,1,0:T(8,128)(2,1)S(1)} %pack.2), channel_id=1, replica_groups=mesh['dp'=4,'z8'=8,'zp'=2,'y'=4,'tp'=2] {'y','zp'}, dimensions={0} | all-to-all | bytes 2228224 | tf_op jit(solution)/shard_map/cond/branch_0_fun/all_to_all | solution.py:307
  21.6 0.3 project.2
  22.0 29.6 %all_to_all.30 = bf16[8,8,1664]{2,1,0:T(8,128)(2,1)S(1)} all-to-all(bf16[8,8,1664]{2,1,0:T(8,128)(2,1)S(1)} %bitcast.18), channel_id=1, replica_groups=mesh['dp'=4,'z8'=8,'zp'=2,'y'=4,'tp'=2] {'z8'}, dimensions={0} | all-to-all | bytes 425984 | tf_op jit(solution)/shard_map/all_to_all | solution.py:307
  51.5 0.0 copy-done
  51.5 0.0 copy-done.2
  51.5 0.0 copy-done.3
  51.5 0.0 copy-done.4
  51.6 0.0 copy-done.5
  51.6 1.7 %delta.1 = (f32[2,4,8,4096]{3,2,1,0:T(8,128)S(1)}, bf16[64,512]{1,0:T(8,128)(2,1)S(1)}) custom-call(s32[2]{0:T(128)S(1)} %copy-done.3, bf16[64,1664]{1,0:T(8,128)(2,1)S(1)} %bitcast.12, f32[2,4,8,4096]{3,2,1,0:T(8,128)S(1)} %copy-done, f32[1,8]{1,0:T(1,128)S(1)} %bitcast.14, f32[2,4,8]{2,1,0:T(4,128)S(1)} %copy-done.2, f32[1,64]{1,0:T(1,128)S(1)} %bitcast.15), custom_call_target="tpu_custom_call" | custom-call | tf_op jit(solution)/shard_map/delta/pallas_call | solution.py:276
  53.3 0.0 copy-start.1
  53.3 16.8 %all_to_all.31 = bf16[8,8,512]{2,1,0:T(8,128)(2,1)S(1)} all-to-all(bf16[8,8,512]{2,1,0:T(8,128)(2,1)S(1)} %bitcast.13), channel_id=1, replica_groups=mesh['dp'=4,'z8'=8,'zp'=2,'y'=4,'tp'=2] {'z8'}, dimensions={0} | all-to-all | bytes 131072 | tf_op jit(solution)/shard_map/all_to_all | solution.py:307
  70.0 0.2 conditional.3
  70.0 0.2 mix.2
  70.3 11.5 %all_to_all.32.x_ref = bf16[16,16,128]{2,1,0:T(8,128)(2,1)S(1)} all-to-all(bf16[16,16,128]{2,1,0:T(8,128)(2,1)S(1)} %get-tuple-element.84), channel_id=1, replica_groups=mesh['dp'=4,'z8'=8,'zp'=2,'y'=4,'tp'=2] {'tp','y','zp'}, dimensions={0} | all-to-all | bytes 131072 | tf_op jit(solution)/shard_map/all_to_all | solution.py:307
  81.8 0.0 copy-done.1
  81.8 1.6 %place.1 = (bf16[4,32,128]{2,1,0:T(8,128)(2,1)}, f32[2,4,8,4096]{3,2,1,0:T(8,128)}) custom-call(bf16[16,16,128]{2,1,0:T(8,128)(2,1)S(1)} %all_to_all.32.x_ref, bf16[512,512]{1,0:T(8,128)(2,1)S(1)} %copy-done.1, f32[2,4,8,4096]{3,2,1,0:T(8,128)S(1)} %get-tuple-element.76.states_ref), custom_call_target="tpu_custom_call" | custom-call | tf_op jit(solution)/shard_map/place/pallas_call | solution.py:276
Async XLA Ops:
  0.6 50.9 %copy-start = (f32[2,4,8,4096]{3,2,1,0:T(8,128)S(1)}, f32[2,4,8,4096]{3,2,1,0:T(8,128)}, u32[]{:S(2)}) copy-start(f32[2,4,8,4096]{3,2,1,0:T(8,128)} %prior_ref.1) | copy-start | bytes 3145732
  0.7 50.9 %copy-start.2 = (f32[2,4,8]{2,1,0:T(4,128)S(1)}, f32[2,4,8]{2,1,0:T(4,128)}, u32[]{:S(2)}) copy-start(f32[2,4,8]{2,1,0:T(4,128)} %extra_ref.1) | copy-start | bytes 772
  0.7 50.9 %copy-start.3 = (s32[2]{0:T(128)S(1)}, s32[2]{0:T(128)}, u32[]{:S(2)}) copy-start(s32[2]{0:T(128)} %accepted_ref.1) | copy-start | bytes 28
  0.7 50.9 %copy-start.4 = (f32[8]{0:T(128)S(1)}, f32[8]{0:T(128)}, u32[]{:S(2)}) copy-start(f32[8]{0:T(128)} %param.25) | copy-start | bytes 100
  0.7 50.9 %copy-start.5 = (f32[64]{0:T(128)S(1)}, f32[64]{0:T(128)}, u32[]{:S(2)}) copy-start(f32[64]{0:T(128)} %param.29) | copy-start | bytes 772
  53.3 28.5 %copy-start.1 = (bf16[512,512]{1,0:T(8,128)(2,1)S(1)}, bf16[512,512]{1,0:T(8,128)(2,1)}, u32[]{:S(2)}) copy-start(bf16[512,512]{1,0:T(8,128)(2,1)} %constant.12.clone.back_ref) | copy-start | bytes 1572868
